TPU v7x, 256 devices: a whole 4x4x8 slice. The times are simulated.
256 devices in a mesh: sp: 16 (over y, x), dp: 16 (over z, core).
Axes of the slice: x: 4, y: 4, z: 8, core: 2. Of those that a mesh axis runs over, the one named last changes fastest.
Arguments:
- tokens: bfloat16 [16, 2048, 2048], P('dp', 'sp'), may hold values from -6 to 6
- query_weight: bfloat16 [2048, 1024], P('dp'), may hold values from -0.125 to 0.125
- key_weight: bfloat16 [2048, 1024], P('dp'), may hold values from -0.125 to 0.125
- value_weight: bfloat16 [2048, 2048], P('dp'), may hold values from -0.125 to 0.125
- output_weight: bfloat16 [2048, 2048], P('dp'), may hold values from -0.125 to 0.125
- log_decay: float32 [2, 16], P(None, 'sp'), may hold values from -0.04 to 0, as said below
Outputs:
- mixed: bfloat16 [16, 2048, 2048], P('dp', 'sp')
Inputs may be any that keep to these rules, and one draw needn't show every extreme that they name: `log_decay`: every entry is negative: the logarithm of a head's decay per position.
All inputs are finite; a program needn't handle non-finite values.
Results may differ from a plain program's by a relative error of at most 0.012.
Values may be sent and summed in bfloat16 or wider, within the bound.
A program may use at most 128 MiB of HBM per device.

v0:
```python
import jax
import jax.numpy as jnp
from jax import lax
from jax.sharding import PartitionSpec as P

HEADS = 16
DK = 64
DV = 128
BLOCK = 512


def in_order(pieces, dim):
    lengths = list(pieces.shape[1:])
    lengths[dim] *= pieces.shape[0]
    return jnp.moveaxis(pieces, 0, dim).reshape(lengths)


def copy_for_each(shard, axis):
    count = lax.axis_size(axis)
    return lax.all_to_all(
        jnp.broadcast_to(shard[None], (count, *shard.shape)), axis, 0, 0, tiled=True
    )


def gathered_copies(shard, axis, dim):
    return in_order(copy_for_each(shard, axis), dim)


def rotate(values_part, positions):
    half_dim = values_part.shape[-1] // 2
    frequency = 10000.0 ** (-jnp.arange(half_dim, dtype=jnp.float32) / half_dim)
    angles = positions[:, None] * frequency[None, :]
    cosine = jnp.cos(angles)[:, None, :]
    sine_part = jnp.sin(angles)[:, None, :]
    first = values_part[..., :half_dim]
    second = values_part[..., half_dim:]
    return jnp.concatenate(
        [first * cosine - second * sine_part, first * sine_part + second * cosine], axis=-1
    )


def retain(query, key_rows, value_rows, log_rate):
    length, heads, key_dim = query.shape
    value_dim = value_rows.shape[-1]
    count = length // BLOCK
    offsets = jnp.arange(BLOCK, dtype=jnp.float32)
    distance = offsets[:, None] - offsets[None, :]
    decay_inner = jnp.where(
        distance[None] >= 0.0,
        jnp.exp(log_rate[:, None, None] * jnp.maximum(distance, 0.0)[None]),
        0.0,
    )
    decay_query = jnp.exp((offsets[:, None] + 1.0) * log_rate[None, :])[:, :, None]
    decay_key = jnp.exp((BLOCK - 1.0 - offsets)[:, None] * log_rate[None, :])[:, :, None]
    decay_block = jnp.exp(BLOCK * log_rate)[:, None, None]

    def blocks(array):
        return array.reshape(count, BLOCK, heads, array.shape[-1])

    def advance(state, inputs):
        query_block, key_block, value_block = inputs
        inner = (
            jnp.einsum("ihd,jhd->hij", query_block, key_block, preferred_element_type=jnp.float32)
            * decay_inner
        )
        result = jnp.einsum(
            "hij,jhv->ihv",
            inner.astype(jnp.bfloat16),
            value_block,
            preferred_element_type=jnp.float32,
        )
        query_wide = query_block.astype(jnp.float32) * decay_query
        result = result + jnp.einsum("ihd,hdv->ihv", query_wide, state)
        key_wide = key_block.astype(jnp.float32) * decay_key
        state = state * decay_block + jnp.einsum(
            "jhd,jhv->hdv", key_wide, value_block.astype(jnp.float32)
        )
        return (state, result)

    initial = jnp.zeros((heads, key_dim, value_dim), jnp.float32)
    final_state, outputs = lax.scan(
        advance, initial, (blocks(query), blocks(key_rows), blocks(value_rows))
    )
    return outputs.reshape(length, heads, value_dim)


def mechanism(stacked, log_decay):
    length = stacked.shape[0]
    widened = stacked[..., : 2 * DK].astype(jnp.float32)
    positions = jnp.arange(length, dtype=jnp.float32)
    query = rotate(widened[..., :DK], positions).astype(jnp.bfloat16)
    key_rows = rotate(widened[..., DK : 2 * DK], positions).astype(jnp.bfloat16)
    value_rows = stacked[..., 2 * DK :]
    forward = retain(query, key_rows, value_rows, log_decay[0])
    backward = retain(
        jnp.flip(query, 0), jnp.flip(key_rows, 0), jnp.flip(value_rows, 0), log_decay[1]
    )
    combined = forward + jnp.flip(backward, 0)
    average = jnp.mean(combined, axis=-1, keepdims=True)
    centred = combined - average
    variance = jnp.mean(centred * centred, axis=-1, keepdims=True)
    return (centred * lax.rsqrt(variance + 1e-06)).astype(jnp.bfloat16)


def shards(tokens, query_weight, key_weight, value_weight, output_weight, log_decay):
    rows = tokens[0]
    row_count = rows.shape[0]
    local_heads = log_decay.shape[1]
    first_head = lax.axis_index("sp") * local_heads
    own_slices = jnp.concatenate(
        [
            lax.dynamic_slice_in_dim(query_weight, first_head * DK, local_heads * DK, 1),
            lax.dynamic_slice_in_dim(key_weight, first_head * DK, local_heads * DK, 1),
            lax.dynamic_slice_in_dim(value_weight, first_head * DV, local_heads * DV, 1),
        ],
        axis=1,
    )
    own_whole = gathered_copies(own_slices, "dp", 0)
    piece = lax.all_gather(rows, "sp", axis=0, tiled=True)
    count = piece.shape[0]
    product = jnp.dot(piece, own_whole, preferred_element_type=jnp.float32).astype(jnp.bfloat16)
    query_part = product[:, : local_heads * DK].reshape(count, local_heads, DK)
    key_part = product[:, local_heads * DK : 2 * local_heads * DK].reshape(count, local_heads, DK)
    value_part = product[:, 2 * local_heads * DK :].reshape(count, local_heads, DV)
    gathered = jnp.concatenate([query_part, key_part, value_part], axis=2)
    normed = mechanism(gathered, log_decay)
    by_token = lax.all_to_all(normed, "sp", split_axis=0, concat_axis=1, tiled=True).reshape(
        row_count, HEADS * DV
    )
    mixed = jnp.dot(
        by_token,
        lax.all_gather(output_weight, "dp", axis=0, tiled=True),
        preferred_element_type=jnp.float32,
    )
    return mixed.astype(jnp.bfloat16)[None]


def solution(mesh):
    placed = (
        P("dp", "sp", None),
        P("dp", None),
        P("dp", None),
        P("dp", None),
        P("dp", None),
        P(None, "sp"),
    )
    return jax.shard_map(
        shards, mesh=mesh, in_specs=placed, out_specs=P("dp", "sp", None), check_vma=False
    )
```

profile of v0, /device:TPU:1, one launch (start us, length us, event | category | flops | bytes accessed | tf_op | source)
XLA Modules:
  0.0 171.0 jit_solution(11749039148471384118)
XLA Ops:
  9.0 1.1 broadcast_in_dim.18
  10.1 10.0 %all-to-all-start = ((bf16[16,128,256]{2,1,0:T(8,128)(2,1)}), bf16[16,128,256]{2,1,0:T(8,128)(2,1)S(1)}, u32[]{:S(2)}, u32[]{:S(2)}) async-start(bf16[16,128,256]{2,1,0:T(8,128)(2,1)} %broadcast_in_dim.18), calls=%async_computation | async-start | bytes 2097152 | tf_op jit(solution)/shard_map/all_to_all | solution.py:20
  20.1 1.4 fusion.116
  22.9 25.2 %all-to-all-done = bf16[16,128,256]{2,1,0:T(8,128)(2,1)S(1)} async-done(((bf16[16,128,256]{2,1,0:T(8,128)(2,1)}), bf16[16,128,256]{2,1,0:T(8,128)(2,1)S(1)}, u32[]{:S(2)}, u32[]{:S(2)}) %all-to-all-start) | async-done | bytes 1048608 | tf_op jit(solution)/shard_map/all_to_all | solution.py:20
  48.1 41.2 %all-gather.6.cloned.1.call-done = bf16[1,2048,2048]{2,1,0:T(8,128)(2,1)} async-done(((bf16[1,128,2048]{2,1,0:T(8,128)(2,1)}), bf16[1,2048,2048]{2,1,0:T(8,128)(2,1)}) %all-gather.6.cloned.1.call-update) | async-done | bytes 8388624 | tf_op jit(solution)/shard_map/all_gather | solution.py:119
  89.3 5.8 %fusion.109 = bf16[2048,256]{0,1:T(8,128)(2,1)S(1)} fusion(bf16[2048,256]{1,0:T(8,128)(2,1)S(1)} %bitcast.255, bf16[1,2048,2048]{2,1,0:T(8,128)(2,1)} %all-gather.6.cloned.1.call-done), kind=kOutput, calls=%fused_computation.103 | convolution fusion | flops 2148007936 | bytes 10485760 | tf_op jit(solution)/shard_map/dot_general | solution.py:121
  95.1 1.0 copy.52
  96.1 1.6 reverse.3
  97.9 1.2 subtract_convert_fusion
  99.3 1.4 rev.14
  100.7 1.4 rev.13
  103.2 17.2 %while.31 = (s32[]{:T(128)}, f32[1,64,128]{2,1,0:T(8,128)S(1)}, f32[4,512,1,128]{3,1,0,2:T(8,128)S(1)}, f32[1,1,1]{2,1,0:T(1,128)}, bf16[4,512,1,64]{1,3,2,0:T(8...) while((s32[]{:T(128)}, f32[1,64,128]{2,1,0:T(8,128)S(1)}, ...), condition=%wide.region_3.4_spmd.clone.clone.clone, body=%wide.region_2.3_spmd.clone.clone.clone.sunk | while | flops 119506944 | bytes 2469500 | solution.py:81
  103.3 2.2 %fusion.158 = f32[128,512]{1,0:T(8,128)S(1)} fusion(f32[]{:T(128)} %get-tuple-element.508, bf16[4,512,1,128]{3,1,2,0:T(8,128)(2,1)S(1)} %get-tuple-element.506, s32[]{:T(128)} %get-tuple-element.491, bf16[4,512,1,64]{1,3,2,0:T(8,128)(2,1)S(1)} %get-tuple-element.507, bf16[4,512,1,64]{1,3,2,0:T(8,128)(2,1)} %get-tuple-element.505), kind=kOutput, calls=%fused_computation.55.clone.1 | convolution fusion | flops 102498304 | bytes 526336 | tf_op jit(solution)/shard_map/while/body/eval_jaxpr/hij,jhv->ihv/dot_general | solution.py:66
  106.5 1.0 fusion.157
  107.6 2.2 %fusion.158 = f32[128,512]{1,0:T(8,128)S(1)} fusion(f32[]{:T(128)} %get-tuple-element.508, bf16[4,512,1,128]{3,1,2,0:T(8,128)(2,1)S(1)} %get-tuple-element.506, s32[]{:T(128)} %get-tuple-element.491, bf16[4,512,1,64]{1,3,2,0:T(8,128)(2,1)S(1)} %get-tuple-element.507, bf16[4,512,1,64]{1,3,2,0:T(8,128)(2,1)} %get-tuple-element.505), kind=kOutput, calls=%fused_computation.55.clone.1 | convolution fusion | flops 102498304 | bytes 526336 | tf_op jit(solution)/shard_map/while/body/eval_jaxpr/hij,jhv->ihv/dot_general | solution.py:66
  110.9 1.0 fusion.157
  111.9 2.2 %fusion.158 = f32[128,512]{1,0:T(8,128)S(1)} fusion(f32[]{:T(128)} %get-tuple-element.508, bf16[4,512,1,128]{3,1,2,0:T(8,128)(2,1)S(1)} %get-tuple-element.506, s32[]{:T(128)} %get-tuple-element.491, bf16[4,512,1,64]{1,3,2,0:T(8,128)(2,1)S(1)} %get-tuple-element.507, bf16[4,512,1,64]{1,3,2,0:T(8,128)(2,1)} %get-tuple-element.505), kind=kOutput, calls=%fused_computation.55.clone.1 | convolution fusion | flops 102498304 | bytes 526336 | tf_op jit(solution)/shard_map/while/body/eval_jaxpr/hij,jhv->ihv/dot_general | solution.py:66
  115.2 1.0 fusion.157
  116.2 2.2 %fusion.158 = f32[128,512]{1,0:T(8,128)S(1)} fusion(f32[]{:T(128)} %get-tuple-element.508, bf16[4,512,1,128]{3,1,2,0:T(8,128)(2,1)S(1)} %get-tuple-element.506, s32[]{:T(128)} %get-tuple-element.491, bf16[4,512,1,64]{1,3,2,0:T(8,128)(2,1)S(1)} %get-tuple-element.507, bf16[4,512,1,64]{1,3,2,0:T(8,128)(2,1)} %get-tuple-element.505), kind=kOutput, calls=%fused_computation.55.clone.1 | convolution fusion | flops 102498304 | bytes 526336 | tf_op jit(solution)/shard_map/while/body/eval_jaxpr/hij,jhv->ihv/dot_general | solution.py:66
  119.5 1.0 fusion.157
  121.7 17.4 %while.30 = (s32[]{:T(128)}, f32[1,64,128]{2,1,0:T(8,128)S(1)}, f32[4,512,1,128]{3,1,0,2:T(8,128)S(1)}, f32[1,1,1]{2,1,0:T(1,128)}, bf16[4,512,1,64]{1,3,2,0:T(8...) while((s32[]{:T(128)}, f32[1,64,128]{2,1,0:T(8,128)S(1)}, ...), condition=%wide.region_1.2_spmd.clone.clone.clone, body=%wide.region_0.1_spmd.clone.clone.clone.sunk | while | flops 119506944 | bytes 2469500 | solution.py:81
  121.7 2.2 %fusion.148 = f32[128,512]{1,0:T(8,128)S(1)} fusion(f32[]{:T(128)} %get-tuple-element.538, bf16[4,512,1,128]{3,1,2,0:T(8,128)(2,1)} %get-tuple-element.536, s32[]{:T(128)} %get-tuple-element.521, bf16[4,512,1,64]{1,3,2,0:T(8,128)(2,1)S(1)} %get-tuple-element.537, bf16[4,512,1,64]{1,3,2,0:T(8,128)(2,1)} %get-tuple-element.535), kind=kOutput, calls=%fused_computation.8.clone.1 | convolution fusion | flops 102498304 | bytes 526336 | tf_op jit(solution)/shard_map/while/body/eval_jaxpr/hij,jhv->ihv/dot_general | solution.py:66
  125.0 1.1 fusion.147
  126.1 2.2 %fusion.148 = f32[128,512]{1,0:T(8,128)S(1)} fusion(f32[]{:T(128)} %get-tuple-element.538, bf16[4,512,1,128]{3,1,2,0:T(8,128)(2,1)} %get-tuple-element.536, s32[]{:T(128)} %get-tuple-element.521, bf16[4,512,1,64]{1,3,2,0:T(8,128)(2,1)S(1)} %get-tuple-element.537, bf16[4,512,1,64]{1,3,2,0:T(8,128)(2,1)} %get-tuple-element.535), kind=kOutput, calls=%fused_computation.8.clone.1 | convolution fusion | flops 102498304 | bytes 526336 | tf_op jit(solution)/shard_map/while/body/eval_jaxpr/hij,jhv->ihv/dot_general | solution.py:66
  129.3 1.1 fusion.147
  130.4 2.2 %fusion.148 = f32[128,512]{1,0:T(8,128)S(1)} fusion(f32[]{:T(128)} %get-tuple-element.538, bf16[4,512,1,128]{3,1,2,0:T(8,128)(2,1)} %get-tuple-element.536, s32[]{:T(128)} %get-tuple-element.521, bf16[4,512,1,64]{1,3,2,0:T(8,128)(2,1)S(1)} %get-tuple-element.537, bf16[4,512,1,64]{1,3,2,0:T(8,128)(2,1)} %get-tuple-element.535), kind=kOutput, calls=%fused_computation.8.clone.1 | convolution fusion | flops 102498304 | bytes 526336 | tf_op jit(solution)/shard_map/while/body/eval_jaxpr/hij,jhv->ihv/dot_general | solution.py:66
  133.7 1.1 fusion.147
  134.8 2.2 %fusion.148 = f32[128,512]{1,0:T(8,128)S(1)} fusion(f32[]{:T(128)} %get-tuple-element.538, bf16[4,512,1,128]{3,1,2,0:T(8,128)(2,1)} %get-tuple-element.536, s32[]{:T(128)} %get-tuple-element.521, bf16[4,512,1,64]{1,3,2,0:T(8,128)(2,1)S(1)} %get-tuple-element.537, bf16[4,512,1,64]{1,3,2,0:T(8,128)(2,1)} %get-tuple-element.535), kind=kOutput, calls=%fused_computation.8.clone.1 | convolution fusion | flops 102498304 | bytes 526336 | tf_op jit(solution)/shard_map/while/body/eval_jaxpr/hij,jhv->ihv/dot_general | solution.py:66
  138.0 1.1 fusion.147
  141.3 1.0 reduce.2
  142.5 15.3 %all_to_all.20 = bf16[16,2,8192]{2,1,0:T(2,128)(2,1)S(1)} all-to-all(bf16[16,2,8192]{2,1,0:T(2,128)(2,1)S(1)} %reshape.742), channel_id=1, replica_groups=mesh['sp'=16,'dp'=16] {'sp'}, dimensions={0} | all-to-all | bytes 1048576 | tf_op jit(solution)/shard_map/all_to_all | solution.py:127
  158.7 5.5 %fusion.112 = bf16[1,128,2048]{2,1,0:T(8,128)(2,1)} fusion(bf16[128,2048]{0,1:T(8,128)(2,1)S(1)} %bitcast.246, bf16[2048,2048]{1,0:T(8,128)(2,1)} %all-gather.4.cloned.1.call-done), kind=kOutput, calls=%fused_computation.105 | convolution fusion | flops 1074003968 | bytes 9437184 | tf_op jit(solution)/shard_map/dot_general | solution.py:130
  (72 shorter events, 16.5 us)
Async XLA Ops:
  6.5 1.5 copy-start
  6.5 82.8 %all-gather.6.cloned.1.call-start = ((), (), s32[]{:S(2)}) async-start(), calls=%async_computation.3 | async-start | bytes 8912896 | tf_op jit(solution)/shard_map/all_gather | solution.py:119
  7.3 151.4 %all-gather.4.cloned.1.call-start = ((), (), s32[]{:S(2)}) async-start(), calls=%async_computation.2 | async-start | bytes 8912896 | tf_op jit(solution)/shard_map/all_gather | solution.py:132
  10.1 38.0 %all-to-all-start = ((bf16[16,128,256]{2,1,0:T(8,128)(2,1)}), bf16[16,128,256]{2,1,0:T(8,128)(2,1)S(1)}, u32[]{:S(2)}, u32[]{:S(2)}) async-start(bf16[16,128,256]{2,1,0:T(8,128)(2,1)} %broadcast_in_dim.18), calls=%async_computation | async-start | bytes 2097152 | tf_op jit(solution)/shard_map/all_to_all | solution.py:20
Sparse Core Ops, SparseCore 0:
  9.8 79.4 all-gather.5
  91.1 56.1 all-gather.3
where the time goes:
time: 172 us; the launch traced here: 171 us
  waiting for transfers between devices  67.9 us (39%)
  matrix products  39 us (23%)
  blocking collectives  15.3 us (9%)
  between operations  15.1 us (9%)
  local copies, waits for them, and re-layouts  13.2 us (8%)
  other arithmetic  10.2 us (6%)
  starting transfers between devices  10 us (6%)
    all_gather x1, waiting for transfers between devices, shards(): piece = lax.all_gather(rows, 'sp', axis=0, tiled=True)  41.2 us
    all_to_all x1, waiting for transfers between devices, copy_for_each(): lax.all_to_all(jnp.broadcast_to(shard[None], (count, *shard.shape)), axis...  25.2 us
    dot_general x8, matrix products, advance(): jnp.einsum('hij,jhv->ihv', inner.astype(jnp.bfloat16), value_block, prefe...  17.5 us
    all_to_all x1, blocking collectives, shards(): lax.all_to_all(normed, 'sp', split_axis=0, concat_axis=1, tiled=True)  15.3 us
    all_to_all x1, starting transfers between devices, copy_for_each(): lax.all_to_all(jnp.broadcast_to(shard[None], (count, *shard.shape)), axis...  9.97 us
    dot_general x8, matrix products, advance(): jnp.einsum('jhd,jhv->hdv', key_wide, value_block.astype(jnp.float32))  8.42 us
    dot_general x1, matrix products, shards(): jnp.dot(piece, own_whole, preferred_element_type=jnp.float32)  5.77 us
    dot_general x1, matrix products, shards(): jnp.dot(by_token, lax.all_gather(output_weight, 'dp', axis=0, tiled=True)...  5.46 us
  transfers between devices with their start and end apart: 3, of which 2 were waited for; matrix products, arithmetic and copies ran while one was open for 33% of the time, Pallas kernels for 0%

commit v1 on v0

v1 whole, which is shorter than its diff:
```python
import jax
import jax.numpy as jnp
import numpy as np
from jax import lax
from jax.experimental import pallas as pl
from jax.experimental.pallas import tpu as pltpu
from jax.sharding import PartitionSpec as P

D = 2048
HEADS = 16
DK = 64
DV = 128
BLOCK = 512
ROWS = 128
SIDE = 4
RING = 8
OWN = 4
PAIRS = 2
EPS = 1e-6

F32 = jnp.float32
BF16 = jnp.bfloat16


def mod(value, size):
    return lax.rem(value + size, size)


def matmul(a, b):
    return jnp.dot(a, b, preferred_element_type=F32)


def kernel(
    tok_hbm, q_hbm, k_hbm, v_hbm, o_hbm, ld_ref, freq_ref, out_ref,
    tok, wq, wo, rates, acc, cosine, sine, tiles, decay, qr, kr, vb, qs, ks,
    ab, states, carried, ret, ns, nb,
    local_sem, tok_s, tok_r, wq_s, wq_r, wqd_s, wqd_r, wo_s, wo_r,
    wy_s, wy_r, wf_s, wf_r, wod_s, wod_r, st_s, st_r, nb_s, nb_r, ld_s, ld_r,
):
    sp = lax.axis_index("sp")
    dp = lax.axis_index("dp")
    y, x = lax.div(sp, SIDE), lax.rem(sp, SIDE)
    z, c = lax.div(dp, 2), lax.rem(dp, 2)
    right, left, across = mod(x + 1, SIDE), mod(x - 1, SIDE), mod(x + 2, SIDE)
    above, below, facing = mod(y + 1, SIDE), mod(y - 1, SIDE), mod(y + 2, SIDE)

    def at_x(to):
        return (y * SIDE + to, dp)

    def at_y(to):
        return (to * SIDE + x, dp)

    def at_z(to):
        return (sp, to * 2 + c)

    other_core = (sp, z * 2 + (1 - c))
    sends = []

    def send(src, dst, send_sem, recv_sem, to):
        copy = pltpu.make_async_remote_copy(
            src_ref=src, dst_ref=dst, send_sem=send_sem, recv_sem=recv_sem,
            device_id=to, device_id_type=pl.DeviceIdType.MESH,
        )
        copy.start()
        sends.append(copy)

    def arrive(dst, send_sem, recv_sem):
        pltpu.make_async_remote_copy(
            src_ref=dst, dst_ref=dst, send_sem=send_sem, recv_sem=recv_sem,
            device_id=other_core, device_id_type=pl.DeviceIdType.MESH,
        ).wait_recv()

    locals_ = []

    def fetch(src, dst):
        copy = pltpu.make_async_copy(src, dst, local_sem.at[len(locals_)])
        copy.start()
        locals_.append(copy)

    fetch(tok_hbm.at[0], tok.at[x])
    fetch(q_hbm.at[:, pl.ds(pl.multiple_of(x * 256, 256), 256)], wq.at[dp, :, 0:256])
    fetch(k_hbm.at[:, pl.ds(pl.multiple_of(x * 256, 256), 256)], wq.at[dp, :, 256:512])
    fetch(v_hbm.at[:, pl.ds(pl.multiple_of(x * 512, 512), 512)], wq.at[dp, :, 512:1024])
    for part in range(SIDE):
        fetch(o_hbm.at[:, part * 512:(part + 1) * 512], wo.at[part, dp])

    barrier = pltpu.get_barrier_semaphore()
    peers = [(lax.rem(sp + o, SIDE * SIDE), dp) for o in range(1, SIDE * SIDE)]
    peers += [at_z(mod(z + 1, RING)), at_z(mod(z - 1, RING)), other_core]
    for peer in peers:
        pl.semaphore_signal(
            barrier, inc=1, device_id=peer, device_id_type=pl.DeviceIdType.MESH
        )
    pl.semaphore_wait(barrier, len(peers))

    def z_block(direction, step):
        return mod(z - step if direction == 0 else z + step, RING) * 2 + c

    def z_next(direction):
        return mod(z + 1 if direction == 0 else z - 1, RING)

    def half(direction):
        return pl.ds(0, 64) if direction == 0 else pl.ds(64, 64)

    def wq_part(direction, step):
        b = z_block(direction, step)
        return wq.at[b] if step < OWN else wq.at[b, half(direction)]

    def wo_part(direction, step):
        b = z_block(direction, step)
        return wo.at[y, b] if step < OWN else wo.at[y, b, half(direction)]

    def send_wq(step):
        for d in range(2):
            part = wq_part(d, step) if step < 3 else wq.at[z_block(d, step), half(d)]
            send(part, part, wq_s.at[d, step], wq_r.at[d, step], at_z(z_next(d)))

    def wait_wq(step):
        for d in range(2):
            arrive(wq_part(d, step), wq_s.at[d, step - 1], wq_r.at[d, step - 1])

    def send_wo(step):
        for d in range(2):
            part = wo_part(d, step) if step < 3 else wo.at[y, z_block(d, step), half(d)]
            send(part, part, wo_s.at[d, step], wo_r.at[d, step], at_z(z_next(d)))

    def wait_wo(step):
        for d in range(2):
            arrive(wo_part(d, step), wo_s.at[d, step - 1], wo_r.at[d, step - 1])

    def nth_block(n):
        if n == 0:
            return dp
        if n == 7:
            return z_block(0, 4)
        return z_block((n - 1) % 2, (n + 1) // 2)

    def swap_wq(n):
        b = nth_block(n)
        send(wq.at[b], wq.at[b], wqd_s.at[n], wqd_r.at[n], other_core)

    def take_wq(n):
        b = nth_block(n) + 1 - 2 * c
        arrive(wq.at[b], wqd_s.at[n], wqd_r.at[n])

    def swap_wo(n):
        b = nth_block(n)
        send(wo.at[:, b], wo.at[:, b], wod_s.at[n], wod_r.at[n], other_core)

    def take_wo(n):
        b = nth_block(n) + 1 - 2 * c
        arrive(wo.at[:, b], wod_s.at[n], wod_r.at[n])

    def spread_y(n):
        part = wo.at[y, nth_block(n)]
        send(part, part, wy_s.at[n, 0], wy_r.at[n, 0], at_y(above))
        send(part, part, wy_s.at[n, 1], wy_r.at[n, 1], at_y(below))

    def forward_y(n):
        b = nth_block(n)
        arrive(wo.at[below, b], wy_s.at[n, 0], wy_r.at[n, 0])
        arrive(wo.at[above, b], wy_s.at[n, 1], wy_r.at[n, 1])
        up, down = wo.at[below, b, half(0)], wo.at[above, b, half(1)]
        send(up, up, wf_s.at[n, 0], wf_r.at[n, 0], at_y(above))
        send(down, down, wf_s.at[n, 1], wf_r.at[n, 1], at_y(below))

    def finish_y(n):
        b = nth_block(n)
        arrive(wo.at[facing, b, half(0)], wf_s.at[n, 0], wf_r.at[n, 0])
        arrive(wo.at[facing, b, half(1)], wf_s.at[n, 1], wf_r.at[n, 1])
        swap_wo(n)

    locals_[0].wait()
    h0, h1 = pl.ds(0, 64), pl.ds(64, 64)
    send(tok.at[x, h0], tok.at[x, h0], tok_s.at[0], tok_r.at[0], at_x(right))
    send(tok.at[x, h1], tok.at[x, h1], tok_s.at[1], tok_r.at[1], at_x(left))
    send(tok.at[x, h1], tok.at[x, h1], tok_s.at[2], tok_r.at[2], at_x(right))
    send(tok.at[x, h0], tok.at[x, h0], tok_s.at[3], tok_r.at[3], at_x(left))
    for n in (1, 2, 3):
        locals_[n].wait()
    send_wq(0)
    for n in range(4, 8):
        locals_[n].wait()
    send_wo(0)
    swap_wq(0)
    for to in range(SIDE):
        @pl.when(jnp.logical_or(y != x, y != to))
        def _():
            copy = pltpu.make_async_remote_copy(
                src_ref=ld_ref, dst_ref=rates.at[x], send_sem=ld_s.at[to], recv_sem=ld_r.at[x],
                device_id=(to * SIDE + y, dp), device_id_type=pl.DeviceIdType.MESH,
            )
            copy.start()

        @pl.when(jnp.logical_and(y == x, y == to))
        def _():
            pltpu.make_async_copy(ld_ref, rates.at[x], ld_r.at[x]).start()

    swap_wo(0)

    lane = lax.broadcasted_iota(jnp.int32, (1, 128), 1)
    low = lax.rem(lane, 64) < 32
    for part in range(SIDE):
        rows = pl.ds(part * ROWS, ROWS)
        at = (lax.broadcasted_iota(jnp.int32, (ROWS, 128), 0) + (y * BLOCK + part * ROWS)).astype(F32)
        angle = at * freq_ref[...]
        cosine[rows, :] = jnp.cos(angle)
        turned = jnp.sin(angle)
        sine[rows, :] = jnp.where(low, -turned, turned)

    arrive(tok.at[left, h0], tok_s.at[0], tok_r.at[0])
    send(tok.at[left, h0], tok.at[left, h0], tok_s.at[4], tok_r.at[4], at_x(right))
    arrive(tok.at[right, h1], tok_s.at[1], tok_r.at[1])
    send(tok.at[right, h1], tok.at[right, h1], tok_s.at[5], tok_r.at[5], at_x(left))
    wait_wq(1)
    send_wq(1)
    swap_wq(1)
    swap_wq(2)

    for j in range(SIDE):
        arrive(rates.at[j], ld_s.at[j], ld_r.at[j])

    def decay_tiles(h, carry):
        a, b = rates[h, 0:1, :], rates[h, 1:2, :]
        i = lax.broadcasted_iota(jnp.int32, (ROWS, 128), 0)
        j = lax.broadcasted_iota(jnp.int32, (ROWS, 128), 1)
        for m in range(7):
            apart = (i - j + (3 - m) * ROWS).astype(F32)
            rate = jnp.where(apart >= 0.0, a, b)
            value = jnp.exp(rate * jnp.abs(apart))
            tiles[h, :, m * 128:(m + 1) * 128] = jnp.where(apart == 0.0, 2.0, value)
        return carry

    lax.fori_loop(0, OWN, decay_tiles, 0)

    first_head = lane < 64

    def decay_rows(p, carry):
        a = jnp.where(first_head, rates[2 * p, 0:1, :], rates[2 * p + 1, 0:1, :])
        b = jnp.where(first_head, rates[2 * p, 1:2, :], rates[2 * p + 1, 1:2, :])
        t = lax.broadcasted_iota(jnp.int32, (BLOCK, 128), 0).astype(F32)
        decay[p, 0] = jnp.exp((t + 1.0) * a)
        decay[p, 1] = jnp.exp((BLOCK - t) * b)
        decay[p, 2] = jnp.exp((BLOCK - 1.0 - t) * a)
        decay[p, 3] = jnp.exp(t * b)
        return carry

    lax.fori_loop(0, PAIRS, decay_rows, 0)

    wait_wo(1)
    send_wo(1)
    spread_y(1)
    spread_y(2)
    wait_wq(2)
    send_wq(2)
    swap_wq(3)
    swap_wq(4)
    forward_y(1)
    forward_y(2)
    wait_wo(2)
    send_wo(2)
    spread_y(3)
    spread_y(4)

    arrive(tok.at[left, h1], tok_s.at[2], tok_r.at[2])
    arrive(tok.at[right, h0], tok_s.at[3], tok_r.at[3])
    arrive(tok.at[across, h0], tok_s.at[4], tok_r.at[4])
    arrive(tok.at[across, h1], tok_s.at[5], tok_r.at[5])

    def project(at, fresh):
        rows = tok[:, :, pl.ds(pl.multiple_of(at * 256, 256), 256)].reshape(BLOCK, 256)
        for n in range(4):
            cols = slice(n * 256, (n + 1) * 256)
            weight = wq[pl.ds(at * 2, 2), :, cols].reshape(256, 256)
            part = matmul(rows, weight)
            acc[:, cols] = part if fresh else acc[:, cols] + part

    for n in range(5):
        take_wq(n)
    project(z, True)

    def project_offset(offset):
        project(mod(z + offset, RING), False)

    def project_many(first, count, stride):
        def step(i, carry):
            project_offset(first + i * stride)
            return carry
        lax.fori_loop(0, count, step, 0)

    project_many(1, 2, 1)
    project_many(6, 2, 1)
    wait_wq(3)
    send_wq(3)
    swap_wq(5)
    swap_wq(6)
    finish_y(1)
    finish_y(2)
    take_wq(5)
    take_wq(6)
    project_many(3, 2, 2)
    forward_y(3)
    forward_y(4)
    wait_wq(4)
    swap_wq(7)
    take_wq(7)
    project_offset(4)

    def turn(cols):
        flat = acc[:, cols].astype(BF16).astype(F32)
        partner = jnp.where(low, pltpu.roll(flat, 96, 1), pltpu.roll(flat, 32, 1))
        return (flat * cosine[...] + partner * sine[...]).astype(BF16)

    row_low = lax.broadcasted_iota(jnp.int32, (128, 1), 0) < 64
    for p in range(PAIRS):
        rq = turn(slice(p * 128, (p + 1) * 128))
        rk = turn(slice(256 + p * 128, 256 + (p + 1) * 128))
        qr[p] = rq
        kr[p] = rk
        value = acc[:, 512 + p * 256:512 + (p + 1) * 256].astype(BF16)
        vb[2 * p] = value[:, :128]
        vb[2 * p + 1] = value[:, 128:]
        wide_q, wide_k = rq.astype(F32), rk.astype(F32)
        qs[p, :, 0:128] = (wide_q * decay[p, 0]).astype(BF16)
        qs[p, :, 128:256] = (wide_q * decay[p, 1]).astype(BF16)
        ks[:, 0:128] = (wide_k * decay[p, 2]).astype(BF16)
        ks[:, 128:256] = (wide_k * decay[p, 3]).astype(BF16)
        both = lax.dot_general(
            ks[...], value, (((0,), (0,)), ((), ())), preferred_element_type=F32
        )
        for d in range(2):
            square = both[d * 128:(d + 1) * 128]
            ab[d, p] = jnp.where(row_low, square[:, :128], square[:, 128:]).astype(BF16)

    for n, to in enumerate((above, below, facing)):
        which = jnp.where(to > y, 0, 1)
        send(ab.at[which], states.at[y], st_s.at[n], st_r.at[n], at_y(to))

    wait_wo(3)
    send_wo(3)
    spread_y(5)
    spread_y(6)

    def in_block(r):
        rows = pl.ds(pl.multiple_of(r * ROWS, ROWS) if not isinstance(r, int) else r * ROWS, ROWS)
        cols = pl.ds(pl.multiple_of((3 - r) * 128, 128), BLOCK)
        for h in range(OWN):
            query = jnp.where((lane >= 64) == (h % 2 == 1), qr[h // 2, rows, :], jnp.zeros((), BF16))
            scores = lax.dot_general(
                query, kr[h // 2], (((1,), (1,)), ((), ())), preferred_element_type=F32
            )
            scores = (scores * tiles[h, :, cols]).astype(BF16)
            ret[r, :, h * 128:(h + 1) * 128] = matmul(scores, vb[h])

    in_block(0)
    in_block(1)
    finish_y(3)
    finish_y(4)
    wait_wo(4)
    spread_y(7)
    in_block(2)
    forward_y(5)
    forward_y(6)
    in_block(3)

    arrive(states.at[below], st_s.at[0], st_r.at[0])
    arrive(states.at[above], st_s.at[1], st_r.at[1])
    arrive(states.at[facing], st_s.at[2], st_r.at[2])
    for p in range(PAIRS):
        for d in range(2):
            rate = jnp.where(row_low, rates[2 * p, d:d + 1, 0:1], rates[2 * p + 1, d:d + 1, 0:1])
            total = jnp.zeros((128, 128), F32)
            for o in range(1, SIDE):
                source = mod(y - o if d == 0 else y + o, SIDE)
                there = (y - o >= 0) if d == 0 else (y + o < SIDE)
                weight = jnp.exp(rate * (BLOCK * (o - 1.0)))
                total = total + jnp.where(there, weight * states[source, p].astype(F32), 0.0)
            total = total.astype(BF16)
            zero = jnp.zeros((), BF16)
            carried[p, d * 128:(d + 1) * 128, 0:128] = jnp.where(row_low, total, zero)
            carried[p, d * 128:(d + 1) * 128, 128:256] = jnp.where(row_low, zero, total)

    def finish_rows(r, dst):
        for p in range(PAIRS):
            rows = pl.ds(pl.multiple_of(r * ROWS, ROWS) if not isinstance(r, int) else r * ROWS, ROWS)
            outside = matmul(qs[p, rows, :], carried[p])
            for e in range(2):
                h = 2 * p + e
                whole = ret[r, :, h * 128:(h + 1) * 128] + outside[:, e * 128:(e + 1) * 128]
                centred = whole - jnp.mean(whole, axis=-1, keepdims=True)
                var = jnp.mean(centred * centred, axis=-1, keepdims=True)
                dst[:, h * 128:(h + 1) * 128] = (centred * lax.rsqrt(var + EPS)).astype(BF16)

    for n, to in enumerate((across, left, right)):
        finish_rows(to, ns.at[n])
        send(ns.at[n], nb.at[x], nb_s.at[n], nb_r.at[n], at_x(to))
    finish_rows(x, nb.at[x])

    finish_y(5)
    finish_y(6)
    forward_y(7)
    finish_y(7)
    for n in range(8):
        take_wo(n)
    arrive(nb.at[across], nb_s.at[0], nb_r.at[0])
    arrive(nb.at[right], nb_s.at[1], nb_r.at[1])
    arrive(nb.at[left], nb_s.at[2], nb_r.at[2])

    for part in range(SIDE):
        total = jnp.zeros((ROWS, 512), F32)
        for g in range(SIDE):
            total = total + matmul(nb[g], wo[part, g * 4:(g + 1) * 4].reshape(512, 512))
        out_ref[0, :, part * 512:(part + 1) * 512] = total.astype(BF16)

    for copy in sends:
        copy.wait_send()
    for to in range(SIDE):
        @pl.when(jnp.logical_or(y != x, y != to))
        def _():
            pltpu.make_async_remote_copy(
                src_ref=ld_ref, dst_ref=rates.at[x], send_sem=ld_s.at[to], recv_sem=ld_r.at[x],
                device_id=(to * SIDE + y, dp), device_id_type=pl.DeviceIdType.MESH,
            ).wait_send()


def shards(tokens, query_weight, key_weight, value_weight, output_weight, log_decay):
    half_dim = DK // 2
    frequency = (
        np.float32(10000.0) ** (-np.arange(half_dim, dtype=np.float32) / np.float32(half_dim))
    ).astype(np.float32)
    frequency = jnp.asarray(np.tile(frequency, 4)[None, :])
    rate = jnp.broadcast_to(jnp.pad(log_decay, ((0, 6), (0, 0))), (8, 128))
    anywhere = pl.BlockSpec(memory_space=pl.ANY)
    vmem = pl.BlockSpec(memory_space=pltpu.VMEM)
    dma = pltpu.SemaphoreType.DMA
    return pl.pallas_call(
        kernel,
        out_shape=jax.ShapeDtypeStruct((1, ROWS, D), BF16),
        in_specs=[anywhere] * 5 + [vmem] * 2,
        out_specs=vmem,
        scratch_shapes=[
            pltpu.VMEM((SIDE, ROWS, D), BF16),
            pltpu.VMEM((16, 128, 1024), BF16),
            pltpu.VMEM((SIDE, 16, 128, 512), BF16),
            pltpu.VMEM((SIDE, 8, 128), F32),
            pltpu.VMEM((BLOCK, 1024), F32),
            pltpu.VMEM((BLOCK, 128), F32),
            pltpu.VMEM((BLOCK, 128), F32),
            pltpu.VMEM((OWN, ROWS, 7 * 128), F32),
            pltpu.VMEM((PAIRS, 4, BLOCK, 128), F32),
            pltpu.VMEM((PAIRS, BLOCK, 128), BF16),
            pltpu.VMEM((PAIRS, BLOCK, 128), BF16),
            pltpu.VMEM((OWN, BLOCK, 128), BF16),
            pltpu.VMEM((PAIRS, BLOCK, 256), BF16),
            pltpu.VMEM((BLOCK, 256), BF16),
            pltpu.VMEM((2, PAIRS, 128, 128), BF16),
            pltpu.VMEM((SIDE, PAIRS, 128, 128), BF16),
            pltpu.VMEM((PAIRS, 256, 256), BF16),
            pltpu.VMEM((SIDE, ROWS, 512), F32),
            pltpu.VMEM((3, ROWS, 512), BF16),
            pltpu.VMEM((SIDE, ROWS, 512), BF16),
            dma((8,)), dma((6,)), dma((6,)),
            dma((2, 4)), dma((2, 4)), dma((8,)), dma((8,)),
            dma((2, 4)), dma((2, 4)),
            dma((8, 2)), dma((8, 2)), dma((8, 2)), dma((8, 2)), dma((8,)), dma((8,)),
            dma((3,)), dma((3,)), dma((3,)), dma((3,)), dma((4,)), dma((4,)),
        ],
        compiler_params=pltpu.CompilerParams(
            collective_id=0, has_side_effects=True, vmem_limit_bytes=60 * 1024 * 1024
        ),
        name="retention",
    )(
        tokens, query_weight, key_weight, value_weight, output_weight, rate, frequency
    )


def solution(mesh):
    placed = (
        P("dp", "sp", None),
        P("dp", None),
        P("dp", None),
        P("dp", None),
        P("dp", None),
        P(None, "sp"),
    )
    return jax.shard_map(
        shards, mesh=mesh, in_specs=placed, out_specs=P("dp", "sp", None), check_vma=False
    )
```

time: 172 us -> 74.8 us (0.43)
  Pallas kernels: 0 us -> 71.5 us
  waiting for transfers between devices: 67.9 us -> 0 us
  matrix products: 39 us -> 0 us
  blocking collectives: 15.3 us -> 0 us
  between operations: 15.1 us -> 0.01 us
  other arithmetic: 10.2 us -> 0 us
  local copies, waits for them, and re-layouts: 13.2 us -> 3.2 us
  starting transfers between devices: 10 us -> 0 us
    pallas_call x0 -> x1, Pallas kernels: none -> 71.5 us  [shards(): pl.pallas_call(kernel, out_shape=jax.ShapeDtypeStruct((1, ROWS, D), BF16)...]
    all_gather x2 -> x0, waiting for transfers between devices: 41.3 us -> none  [the longest x1 41.2 us: shards(): piece = lax.all_gather(rows, 'sp', axis=0, tiled=True)]
    dot_general x26 -> x0, matrix products: 39 us -> none  [the longest x8 17.5 us: advance(): jnp.einsum('hij,jhv->ihv', inner.astype(jnp.bfloat16), value_block, prefe...]
    all_to_all x1 -> x0, waiting for transfers between devices: 25.2 us -> none  [copy_for_each(): lax.all_to_all(jnp.broadcast_to(shard[None], (count, *shard.shape)), axis...]
    all_to_all x1 -> x0, blocking collectives: 15.3 us -> none  [shards(): lax.all_to_all(normed, 'sp', split_axis=0, concat_axis=1, tiled=True)]
    all_to_all x1 -> x0, starting transfers between devices: 9.97 us -> none  [copy_for_each(): lax.all_to_all(jnp.broadcast_to(shard[None], (count, *shard.shape)), axis...]
    exp x8 -> x0, other arithmetic: 5.31 us -> none  [retain(): jnp.exp((offsets[:, None] + 1.0) * log_rate[None, :])[:, :, None]]
    rev x3 -> x0, local copies, waits for them, and re-layouts: 3.19 us -> none  [the longest x1 1.4 us: mechanism(): jnp.flip(query, 0)]
  transfers between devices with their start and end apart: 3 -> 0, of which waited for: 2 -> 0; matrix products, arithmetic and copies ran while one was open for 33% -> 0% of each run, Pallas kernels for 0% -> 0%
where the time goes in v1:
time: 74.8 us; the launch traced here: 74.7 us
  Pallas kernels  71.5 us (96%)
  local copies, waits for them, and re-layouts  3.2 us (4%)
    pallas_call x1, Pallas kernels, shards(): pl.pallas_call(kernel, out_shape=jax.ShapeDtypeStruct((1, ROWS, D), BF16)...  71.5 us
    unnamed x1, local copies, waits for them, and re-layouts  1.88 us

profile of v1, /device:TPU:1, one launch (start us, length us, event | category | flops | bytes accessed | tf_op | source)
XLA Modules:
  0.0 74.7 jit_solution(13244837642081867099)
XLA Ops:
  0.0 0.7 pad_bitcast_fusion
  0.7 0.7 broadcast_in_dim.8.ld_ref
  1.3 71.5 %retention.1 = bf16[1,128,2048]{2,1,0:T(8,128)(2,1)} custom-call(bf16[1,128,2048]{2,1,0:T(8,128)(2,1)} %tok_hbm.1, bf16[128,1024]{1,0:T(8,128)(2,1)} %q_hbm.1, bf16[128,1024]{1,0:T(8,128)(2,1)} %k_hbm.1, bf16[128,2048]{1,0:T(8,128)(2,1)} %v_hbm.1, bf16[128,2048]{1,0:T(8,128)(2,1)} %o_hbm.1, f32[8,128]{1,0:T(8,128)} %broadcast_in_dim.8.ld_ref, ...), custom_call_target="tpu_custom_call" | custom-call | tf_op jit(solution)/shard_map/retention/pallas_call | solution.py:436
  72.8 1.9 %copy.9 = bf16[1,128,2048]{2,1,0:T(8,128)(2,1)} copy(bf16[1,128,2048]{2,1,0:T(8,128)(2,1)} %retention.1) | data formatting | bytes 1048576

commit v2 on v0

v2 whole, which is shorter than its diff:
```python
import jax
import jax.numpy as jnp
import numpy as np
from jax import lax
from jax.experimental import pallas as pl
from jax.experimental.pallas import tpu as pltpu
from jax.sharding import PartitionSpec as P

D = 2048
HEADS = 16
DK = 64
DV = 128
BLOCK = 512
ROWS = 128
SIDE = 4
RING = 8
OWN = 4
PAIRS = 2
EPS = 1e-6
KV = 768

F32 = jnp.float32
BF16 = jnp.bfloat16


def mod(value, size):
    return lax.rem(value + size, size)


def matmul(a, b):
    return jnp.dot(a, b, preferred_element_type=F32)


def kernel(
    tok_hbm, q_hbm, k_hbm, v_hbm, o_hbm, ld_ref, freq_ref, out_ref,
    tok, wq, wk, wo, own_rate, rates, acc_q, acc_k, cosine, sine, tiles, decay, qr, kr, vb, qs, ks,
    ab, states, carried, ret, ns, relay, nb, acc_o,
    local_sem, tok_s, tok_r, wq_s, wq_r, wqd_s, wqd_r, wk_s, wk_r, wkd_s, wkd_r, wo_s, wo_r,
    wy_s, wy_r, wf_s, wf_r, wod_s, wod_r, own_s, own_r, st_s, st_r, nb_s, nb_r, ld_s, ld_r,
):
    sp = lax.axis_index("sp")
    dp = lax.axis_index("dp")
    y, x = lax.div(sp, SIDE), lax.rem(sp, SIDE)
    z, c = lax.div(dp, 2), lax.rem(dp, 2)
    right, left, across = mod(x + 1, SIDE), mod(x - 1, SIDE), mod(x + 2, SIDE)
    above, below, facing = mod(y + 1, SIDE), mod(y - 1, SIDE), mod(y + 2, SIDE)
    h0, h1 = pl.ds(0, 64), pl.ds(64, 64)

    def at_x(to):
        return (y * SIDE + to, dp)

    def at_y(to):
        return (to * SIDE + x, dp)

    def at_z(to):
        return (sp, to * 2 + c)

    other_core = (sp, z * 2 + (1 - c))
    sends = []

    def send(src, dst, send_sem, recv_sem, to):
        copy = pltpu.make_async_remote_copy(
            src_ref=src, dst_ref=dst, send_sem=send_sem, recv_sem=recv_sem,
            device_id=to, device_id_type=pl.DeviceIdType.MESH,
        )
        copy.start()
        sends.append(copy)

    def arrive(dst, send_sem, recv_sem):
        pltpu.make_async_remote_copy(
            src_ref=dst, dst_ref=dst, send_sem=send_sem, recv_sem=recv_sem,
            device_id=other_core, device_id_type=pl.DeviceIdType.MESH,
        ).wait_recv()

    fetched = []

    def fetch(src, dst):
        copy = pltpu.make_async_copy(src, dst, local_sem.at[len(fetched)])
        copy.start()
        fetched.append(copy)

    for part in range(SIDE):
        fetch(o_hbm.at[:, part * 512:(part + 1) * 512], wo.at[part, dp])
    fetch(tok_hbm.at[0], tok.at[x])
    fetch(k_hbm.at[:, pl.ds(pl.multiple_of(x * 256, 256), 256)], wk.at[dp, :, 0:256])
    fetch(v_hbm.at[:, pl.ds(pl.multiple_of(x * 512, 512), 512)], wk.at[dp, :, 256:KV])
    fetch(q_hbm.at[:, pl.ds(pl.multiple_of(x * 256, 256), 256)], wq.at[dp])

    sub = lax.broadcasted_iota(jnp.int32, (8, 128), 0)
    own_rate[...] = jnp.where(sub == 0, ld_ref[0:1, 0:1], ld_ref[1:2, 0:1])

    barrier = pltpu.get_barrier_semaphore()
    peers = [(lax.rem(sp + o, SIDE * SIDE), dp) for o in range(1, SIDE * SIDE)]
    peers += [at_z(mod(z + 1, RING)), at_z(mod(z - 1, RING)), other_core]
    for peer in peers:
        pl.semaphore_signal(
            barrier, inc=1, device_id=peer, device_id_type=pl.DeviceIdType.MESH
        )
    pl.semaphore_wait(barrier, len(peers))
    for copy in fetched:
        copy.wait()

    def half(direction):
        return h0 if direction == 0 else h1

    def z_block(direction, step):
        return mod(z - step if direction == 0 else z + step, RING) * 2 + c

    def z_next(direction):
        return mod(z + 1 if direction == 0 else z - 1, RING)

    def nth_block(n):
        if n == 0:
            return dp
        if n == 7:
            return z_block(0, 4)
        return z_block((n - 1) % 2, (n + 1) // 2)

    def nth_other(n):
        return nth_block(n) + 1 - 2 * c

    def blocks_of(step):
        return (0,) if step == 0 else (2 * step - 1, 2 * step) if step < 4 else (7,)

    def ring_wait(view, step, s_sem, r_sem):
        if step > 0:
            for d in range(2):
                b = z_block(d, step)
                arrive(
                    view(b) if step < 4 else view(b, half(d)), s_sem.at[d, step - 1], r_sem.at[d, step - 1]
                )

    def ring_send(view, step, s_sem, r_sem):
        if step < 4:
            for d in range(2):
                b = z_block(d, step)
                part = view(b) if step < 3 else view(b, half(d))
                send(part, part, s_sem.at[d, step], r_sem.at[d, step], at_z(z_next(d)))

    def weight_step(ref, step, s_sem, r_sem, d_s, d_r):
        def view(b, rows=None):
            return ref.at[b] if rows is None else ref.at[b, rows]

        ring_wait(view, step, s_sem, r_sem)
        ring_send(view, step, s_sem, r_sem)
        for n in blocks_of(step):
            b = nth_block(n)
            send(ref.at[b], ref.at[b], d_s.at[n], d_r.at[n], other_core)

    def k_step(step):
        weight_step(wk, step, wk_s, wk_r, wkd_s, wkd_r)

    def q_step(step):
        weight_step(wq, step, wq_s, wq_r, wqd_s, wqd_r)

    def share(part, n, index):
        send(part, part, wod_s.at[n, index], wod_r.at[n, index], other_core)

    def o_step(step):
        def view(b, rows=None):
            return wo.at[y, b] if rows is None else wo.at[y, b, rows]

        ring_wait(view, step, wo_s, wo_r)
        ring_send(view, step, wo_s, wo_r)
        if step > 0:
            for n in blocks_of(step):
                part = wo.at[y, nth_block(n)]
                send(part, part, wy_s.at[n, 0], wy_r.at[n, 0], at_y(above))
                send(part, part, wy_s.at[n, 1], wy_r.at[n, 1], at_y(below))
                share(part, n, 0)

    def f_step(step):
        for n in blocks_of(step):
            b = nth_block(n)
            arrive(wo.at[below, b], wy_s.at[n, 0], wy_r.at[n, 0])
            arrive(wo.at[above, b], wy_s.at[n, 1], wy_r.at[n, 1])
            up, down = wo.at[below, b, h0], wo.at[above, b, h1]
            send(up, up, wf_s.at[n, 0], wf_r.at[n, 0], at_y(above))
            send(down, down, wf_s.at[n, 1], wf_r.at[n, 1], at_y(below))
            share(wo.at[below, b], n, 1)
            share(wo.at[above, b], n, 2)

    def g_step(step):
        for n in blocks_of(step):
            b = nth_block(n)
            arrive(wo.at[facing, b, h0], wf_s.at[n, 0], wf_r.at[n, 0])
            arrive(wo.at[facing, b, h1], wf_s.at[n, 1], wf_r.at[n, 1])
            share(wo.at[facing, b], n, 3)

    def own_output_block():
        send(wo.at[:, dp], wo.at[:, dp], own_s.at[0], own_r.at[0], other_core)

    def take_output(n):
        b = nth_other(n)
        if n == 0:
            arrive(wo.at[:, b], own_s.at[0], own_r.at[0])
        else:
            for index, part in enumerate((y, below, above, facing)):
                arrive(wo.at[part, b], wod_s.at[n, index], wod_r.at[n, index])

    def tokens_first():
        send(tok.at[x, h0], tok.at[x, h0], tok_s.at[0], tok_r.at[0], at_x(right))
        send(tok.at[x, h1], tok.at[x, h1], tok_s.at[1], tok_r.at[1], at_x(left))

    def tokens_second():
        send(tok.at[x, h1], tok.at[x, h1], tok_s.at[2], tok_r.at[2], at_x(right))
        send(tok.at[x, h0], tok.at[x, h0], tok_s.at[3], tok_r.at[3], at_x(left))

    def tokens_forward():
        arrive(tok.at[left, h0], tok_s.at[0], tok_r.at[0])
        send(tok.at[left, h0], tok.at[left, h0], tok_s.at[4], tok_r.at[4], at_x(right))
        arrive(tok.at[right, h1], tok_s.at[1], tok_r.at[1])
        send(tok.at[right, h1], tok.at[right, h1], tok_s.at[5], tok_r.at[5], at_x(left))

    def rate_copy(to):
        return pltpu.make_async_remote_copy(
            src_ref=own_rate, dst_ref=rates.at[x], send_sem=ld_s.at[to], recv_sem=ld_r.at[x],
            device_id=(to * SIDE + y, dp), device_id_type=pl.DeviceIdType.MESH,
        )

    def send_rates():
        for to in range(SIDE):
            @pl.when(jnp.logical_or(y != x, y != to))
            def _():
                rate_copy(to).start()

            @pl.when(jnp.logical_and(y == x, y == to))
            def _():
                pltpu.make_async_copy(own_rate, rates.at[x], ld_r.at[x]).start()

    lane = lax.broadcasted_iota(jnp.int32, (1, 128), 1)
    low = lax.rem(lane, 64) < 32

    def tables():
        for part in range(SIDE):
            rows = pl.ds(part * ROWS, ROWS)
            at = lax.broadcasted_iota(jnp.int32, (ROWS, 128), 0) + (y * BLOCK + part * ROWS)
            angle = at.astype(F32) * freq_ref[...]
            cosine[rows, :] = jnp.cos(angle)
            turned = jnp.sin(angle)
            sine[rows, :] = jnp.where(low, -turned, turned)

    def decays():
        for j in range(SIDE):
            arrive(rates.at[j], ld_s.at[j], ld_r.at[j])

        def decay_tiles(h, carry):
            a, b = rates[h, 0:1, :], rates[h, 1:2, :]
            i = lax.broadcasted_iota(jnp.int32, (ROWS, 128), 0)
            j = lax.broadcasted_iota(jnp.int32, (ROWS, 128), 1)
            for m in range(7):
                apart = (i - j + (3 - m) * ROWS).astype(F32)
                rate = jnp.where(apart >= 0.0, a, b)
                value = jnp.exp(rate * jnp.abs(apart))
                tiles[h, :, m * 128:(m + 1) * 128] = jnp.where(apart == 0.0, 2.0, value)
            return carry

        lax.fori_loop(0, OWN, decay_tiles, 0)
        first_head = lane < 64

        def decay_rows(p, carry):
            a = jnp.where(first_head, rates[2 * p, 0:1, :], rates[2 * p + 1, 0:1, :])
            b = jnp.where(first_head, rates[2 * p, 1:2, :], rates[2 * p + 1, 1:2, :])
            t = lax.broadcasted_iota(jnp.int32, (BLOCK, 128), 0).astype(F32)
            decay[p, 0] = jnp.exp((t + 1.0) * a)
            decay[p, 1] = jnp.exp((BLOCK - t) * b)
            decay[p, 2] = jnp.exp((BLOCK - 1.0 - t) * a)
            decay[p, 3] = jnp.exp(t * b)
            return carry

        lax.fori_loop(0, PAIRS, decay_rows, 0)

    def tokens_all():
        arrive(tok.at[left, h1], tok_s.at[2], tok_r.at[2])
        arrive(tok.at[right, h0], tok_s.at[3], tok_r.at[3])
        arrive(tok.at[across, h0], tok_s.at[4], tok_r.at[4])
        arrive(tok.at[across, h1], tok_s.at[5], tok_r.at[5])

    def project(ref, acc, width, offset, fresh):
        at = mod(z + offset, RING)
        rows = tok[:, :, pl.ds(pl.multiple_of(at * 256, 256), 256)].reshape(BLOCK, 256)
        for n in range(width // 256):
            cols = slice(n * 256, (n + 1) * 256)
            part = matmul(rows, ref[pl.ds(at * 2, 2), :, cols].reshape(256, 256))
            acc[:, cols] = part if fresh else acc[:, cols] + part

    def project_many(ref, acc, width, first, count, stride):
        def step(i, carry):
            project(ref, acc, width, first + i * stride, False)
            return carry

        lax.fori_loop(0, count, step, 0)

    def k_project(stage):
        k_or_q(stage, wk, acc_k, KV, wkd_s, wkd_r)

    def q_project(stage):
        k_or_q(stage, wq, acc_q, 256, wqd_s, wqd_r)

    def k_or_q(stage, ref, acc, width, d_s, d_r):
        for n in ((0, 1, 2), (3, 4), (5, 6), (7,))[stage]:
            arrive(ref.at[nth_other(n)], d_s.at[n], d_r.at[n])
        if stage == 0:
            project(ref, acc, width, 0, True)
            project_many(ref, acc, width, 1, 2, 6)
        elif stage == 3:
            project(ref, acc, width, 4, False)
        else:
            project_many(ref, acc, width, stage + 1, 2, 6 - 2 * stage)

    def turn(flat):
        wide = flat.astype(BF16).astype(F32)
        partner = jnp.where(low, pltpu.roll(wide, 96, 1), pltpu.roll(wide, 32, 1))
        return (wide * cosine[...] + partner * sine[...]).astype(BF16)

    row_low = lax.broadcasted_iota(jnp.int32, (128, 1), 0) < 64

    def keys_values():
        for p in range(PAIRS):
            rk = turn(acc_k[:, p * 128:(p + 1) * 128])
            kr[p] = rk
            value = acc_k[:, 256 + p * 256:256 + (p + 1) * 256].astype(BF16)
            vb[2 * p] = value[:, :128]
            vb[2 * p + 1] = value[:, 128:]
            wide_k = rk.astype(F32)
            ks[:, 0:128] = (wide_k * decay[p, 2]).astype(BF16)
            ks[:, 128:256] = (wide_k * decay[p, 3]).astype(BF16)
            both = lax.dot_general(
                ks[...], value, (((0,), (0,)), ((), ())), preferred_element_type=F32
            )
            for d in range(2):
                square = both[d * 128:(d + 1) * 128]
                ab[d, p] = jnp.where(row_low, square[:, :128], square[:, 128:]).astype(BF16)
        for n, to in ((2, facing), (0, above), (1, below)):
            send(ab.at[jnp.where(to > y, 0, 1)], states.at[y], st_s.at[n], st_r.at[n], at_y(to))

    def queries():
        for p in range(PAIRS):
            rq = turn(acc_q[:, p * 128:(p + 1) * 128])
            qr[p] = rq
            wide_q = rq.astype(F32)
            qs[p, :, 0:128] = (wide_q * decay[p, 0]).astype(BF16)
            qs[p, :, 128:256] = (wide_q * decay[p, 1]).astype(BF16)

    def in_block(r):
        rows = pl.ds(pl.multiple_of(r * ROWS, ROWS), ROWS)
        cols = pl.ds(pl.multiple_of((3 - r) * 128, 128), BLOCK)
        for h in range(OWN):
            query = jnp.where((lane >= 64) == (h % 2 == 1), qr[h // 2, rows, :], jnp.zeros((), BF16))
            scores = lax.dot_general(
                query, kr[h // 2], (((1,), (1,)), ((), ())), preferred_element_type=F32
            )
            scores = (scores * tiles[h, :, cols]).astype(BF16)
            ret[r, :, h * 128:(h + 1) * 128] = matmul(scores, vb[h])

    def carry_states():
        arrive(states.at[below], st_s.at[0], st_r.at[0])
        arrive(states.at[above], st_s.at[1], st_r.at[1])
        arrive(states.at[facing], st_s.at[2], st_r.at[2])
        for p in range(PAIRS):
            for d in range(2):
                rate = jnp.where(row_low, rates[2 * p, d:d + 1, 0:1], rates[2 * p + 1, d:d + 1, 0:1])
                total = jnp.zeros((128, 128), F32)
                for o in range(1, SIDE):
                    source = mod(y - o if d == 0 else y + o, SIDE)
                    there = (y - o >= 0) if d == 0 else (y + o < SIDE)
                    weight = jnp.exp(rate * (BLOCK * (o - 1.0)))
                    total = total + jnp.where(there, weight * states[source, p].astype(F32), 0.0)
                total = total.astype(BF16)
                zero = jnp.zeros((), BF16)
                carried[p, d * 128:(d + 1) * 128, 0:128] = jnp.where(row_low, total, zero)
                carried[p, d * 128:(d + 1) * 128, 128:256] = jnp.where(row_low, zero, total)

    def finish_rows(r, dst):
        rows = pl.ds(pl.multiple_of(r * ROWS, ROWS), ROWS)
        for p in range(PAIRS):
            outside = matmul(qs[p, rows, :], carried[p])
            for e in range(2):
                h = 2 * p + e
                whole = ret[r, :, h * 128:(h + 1) * 128] + outside[:, e * 128:(e + 1) * 128]
                centred = whole - jnp.mean(whole, axis=-1, keepdims=True)
                var = jnp.mean(centred * centred, axis=-1, keepdims=True)
                dst[:, h * 128:(h + 1) * 128] = (centred * lax.rsqrt(var + EPS)).astype(BF16)

    to_rows = (across, left, right, x)

    def normed(n):
        r = to_rows[n]
        if n == 3:
            finish_rows(r, nb.at[x])
            return
        finish_rows(r, ns.at[n])
        if n == 0:
            send(ns.at[0, h0], relay.at[0], nb_s.at[0], nb_r.at[0], at_x(right))
            send(ns.at[0, h1], relay.at[1], nb_s.at[1], nb_r.at[1], at_x(left))
        else:
            send(ns.at[n], nb.at[x], nb_s.at[n + 1], nb_r.at[n + 1], at_x(r))

    def normed_forward():
        arrive(relay.at[0], nb_s.at[0], nb_r.at[0])
        send(relay.at[0], nb.at[left, h0], nb_s.at[4], nb_r.at[4], at_x(right))
        arrive(relay.at[1], nb_s.at[1], nb_r.at[1])
        send(relay.at[1], nb.at[right, h1], nb_s.at[5], nb_r.at[5], at_x(left))

    def normed_all():
        arrive(nb.at[right], nb_s.at[2], nb_r.at[2])
        arrive(nb.at[left], nb_s.at[3], nb_r.at[3])
        arrive(nb.at[across, h0], nb_s.at[4], nb_r.at[4])
        arrive(nb.at[across, h1], nb_s.at[5], nb_r.at[5])

    def output(stage):
        if stage == 0:
            normed_all()
        for n in ((0, 1, 2, 3, 4), (5, 6, 7))[stage]:
            take_output(n)
        for part in range(SIDE):
            cols = slice(part * 512, (part + 1) * 512)
            total = jnp.zeros((ROWS, 512), F32) if stage == 0 else acc_o[:, cols]
            for offset in ((0, 1, 7, 2, 6), (3, 5, 4))[stage]:
                at = mod(z + offset, RING)
                lhs = nb[lax.div(at, 2), :, pl.ds(pl.multiple_of(lax.rem(at, 2) * 256, 256), 256)]
                total = total + matmul(lhs, wo[part, pl.ds(at * 2, 2)].reshape(256, 512))
            if stage == 0:
                acc_o[:, cols] = total
            else:
                out_ref[0, :, cols] = total.astype(BF16)

    def run(name, task, *arguments):
        with jax.named_scope(name):
            task(*arguments)

    run("O0", o_step, 0)
    run("K0", k_step, 0)
    run("T0", tokens_first)
    run("O1", o_step, 1)
    run("TAB", tables)
    run("Q0", q_step, 0)
    run("LD", send_rates)
    run("TF", tokens_forward)
    run("K1", k_step, 1)
    run("T1", tokens_second)
    run("SO0", own_output_block)
    run("DEC", decays)
    run("O2", o_step, 2)
    run("F1", f_step, 1)
    run("K2", k_step, 2)
    run("F2", f_step, 2)
    run("TA", tokens_all)
    run("KA", k_project, 0)
    run("Q1", q_step, 1)
    run("G1", g_step, 1)
    run("QA", q_project, 0)
    run("K3", k_step, 3)
    run("O3", o_step, 3)
    run("Q2", q_step, 2)
    run("KB", k_project, 1)
    run("KC", k_project, 2)
    run("K4", k_step, 4)
    run("KD", k_project, 3)
    run("RK", keys_values)
    run("Q3", q_step, 3)
    run("Q4", q_step, 4)
    run("G2", g_step, 2)
    run("QB", q_project, 1)
    run("QC", q_project, 2)
    run("O4", o_step, 4)
    run("F3", f_step, 3)
    run("QD", q_project, 3)
    run("RQ", queries)
    run("I0", in_block, to_rows[0])
    run("I1", in_block, to_rows[1])
    run("CAR", carry_states)
    run("N0", normed, 0)
    run("I2", in_block, to_rows[2])
    run("N1", normed, 1)
    run("N2", normed, 2)
    run("F4", f_step, 4)
    run("NF", normed_forward)
    run("G3", g_step, 3)
    run("I3", in_block, to_rows[3])
    run("G4", g_step, 4)
    run("N3", normed, 3)
    run("OA", output, 0)
    run("OB", output, 1)
    for copy in sends:
        copy.wait_send()
    for to in range(SIDE):
        @pl.when(jnp.logical_or(y != x, y != to))
        def _():
            rate_copy(to).wait_send()


def shards(tokens, query_weight, key_weight, value_weight, output_weight, log_decay):
    half_dim = DK // 2
    frequency = (
        np.float32(10000.0) ** (-np.arange(half_dim, dtype=np.float32) / np.float32(half_dim))
    ).astype(np.float32)
    frequency = jnp.asarray(np.tile(frequency, 4)[None, :])
    anywhere = pl.BlockSpec(memory_space=pl.ANY)
    vmem = pl.BlockSpec(memory_space=pltpu.VMEM)
    dma = pltpu.SemaphoreType.DMA
    return pl.pallas_call(
        kernel,
        out_shape=jax.ShapeDtypeStruct((1, ROWS, D), BF16),
        in_specs=[anywhere] * 5 + [vmem] * 2,
        out_specs=vmem,
        scratch_shapes=[
            pltpu.VMEM((SIDE, ROWS, D), BF16),
            pltpu.VMEM((16, 128, 256), BF16),
            pltpu.VMEM((16, 128, KV), BF16),
            pltpu.VMEM((SIDE, 16, 128, 512), BF16),
            pltpu.VMEM((8, 128), F32),
            pltpu.VMEM((SIDE, 8, 128), F32),
            pltpu.VMEM((BLOCK, 256), F32),
            pltpu.VMEM((BLOCK, KV), F32),
            pltpu.VMEM((BLOCK, 128), F32),
            pltpu.VMEM((BLOCK, 128), F32),
            pltpu.VMEM((OWN, ROWS, 7 * 128), F32),
            pltpu.VMEM((PAIRS, 4, BLOCK, 128), F32),
            pltpu.VMEM((PAIRS, BLOCK, 128), BF16),
            pltpu.VMEM((PAIRS, BLOCK, 128), BF16),
            pltpu.VMEM((OWN, BLOCK, 128), BF16),
            pltpu.VMEM((PAIRS, BLOCK, 256), BF16),
            pltpu.VMEM((BLOCK, 256), BF16),
            pltpu.VMEM((2, PAIRS, 128, 128), BF16),
            pltpu.VMEM((SIDE, PAIRS, 128, 128), BF16),
            pltpu.VMEM((PAIRS, 256, 256), BF16),
            pltpu.VMEM((SIDE, ROWS, 512), F32),
            pltpu.VMEM((3, ROWS, 512), BF16),
            pltpu.VMEM((2, 64, 512), BF16),
            pltpu.VMEM((SIDE, ROWS, 512), BF16),
            pltpu.VMEM((ROWS, D), F32),
            dma((8,)), dma((6,)), dma((6,)),
            dma((2, 4)), dma((2, 4)), dma((8,)), dma((8,)),
            dma((2, 4)), dma((2, 4)), dma((8,)), dma((8,)),
            dma((2, 4)), dma((2, 4)),
            dma((8, 2)), dma((8, 2)), dma((8, 2)), dma((8, 2)),
            dma((8, 4)), dma((8, 4)), dma((1,)), dma((1,)),
            dma((3,)), dma((3,)), dma((6,)), dma((6,)), dma((4,)), dma((4,)),
        ],
        compiler_params=pltpu.CompilerParams(
            collective_id=0, has_side_effects=True, vmem_limit_bytes=60 * 1024 * 1024
        ),
        name="retention",
    )(
        tokens, query_weight, key_weight, value_weight, output_weight, log_decay, frequency
    )


def solution(mesh):
    placed = (
        P("dp", "sp", None),
        P("dp", None),
        P("dp", None),
        P("dp", None),
        P("dp", None),
        P(None, "sp"),
    )
    return jax.shard_map(
        shards, mesh=mesh, in_specs=placed, out_specs=P("dp", "sp", None), check_vma=False
    )
```

time: 172 us -> 66.7 us (0.39)
  waiting for transfers between devices: 67.9 us -> 0 us
  Pallas kernels: 0 us -> 63.3 us
  matrix products: 39 us -> 0 us
  blocking collectives: 15.3 us -> 0 us
  between operations: 15.1 us -> 0.01 us
  other arithmetic: 10.2 us -> 0 us
  local copies, waits for them, and re-layouts: 13.2 us -> 3.18 us
  starting transfers between devices: 10 us -> 0 us
    pallas_call x0 -> x1, Pallas kernels: none -> 63.3 us  [shards(): pl.pallas_call(kernel, out_shape=jax.ShapeDtypeStruct((1, ROWS, D), BF16)...]
    all_gather x2 -> x0, waiting for transfers between devices: 41.3 us -> none  [the longest x1 41.2 us: shards(): piece = lax.all_gather(rows, 'sp', axis=0, tiled=True)]
    dot_general x26 -> x0, matrix products: 39 us -> none  [the longest x8 17.5 us: advance(): jnp.einsum('hij,jhv->ihv', inner.astype(jnp.bfloat16), value_block, prefe...]
    all_to_all x1 -> x0, waiting for transfers between devices: 25.2 us -> none  [copy_for_each(): lax.all_to_all(jnp.broadcast_to(shard[None], (count, *shard.shape)), axis...]
    all_to_all x1 -> x0, blocking collectives: 15.3 us -> none  [shards(): lax.all_to_all(normed, 'sp', split_axis=0, concat_axis=1, tiled=True)]
    all_to_all x1 -> x0, starting transfers between devices: 9.97 us -> none  [copy_for_each(): lax.all_to_all(jnp.broadcast_to(shard[None], (count, *shard.shape)), axis...]
    exp x8 -> x0, other arithmetic: 5.31 us -> none  [retain(): jnp.exp((offsets[:, None] + 1.0) * log_rate[None, :])[:, :, None]]
    rev x3 -> x0, local copies, waits for them, and re-layouts: 3.19 us -> none  [the longest x1 1.4 us: mechanism(): jnp.flip(query, 0)]
  transfers between devices with their start and end apart: 3 -> 0, of which waited for: 2 -> 0; matrix products, arithmetic and copies ran while one was open for 33% -> 0% of each run, Pallas kernels for 0% -> 0%
where the time goes in v2:
time: 66.7 us; the launch traced here: 66.5 us
  Pallas kernels  63.3 us (95%)
  local copies, waits for them, and re-layouts  3.18 us (5%)
    pallas_call x1, Pallas kernels, shards(): pl.pallas_call(kernel, out_shape=jax.ShapeDtypeStruct((1, ROWS, D), BF16)...  63.3 us
    unnamed x2, local copies, waits for them, and re-layouts  3.18 us

profile of v2, /device:TPU:1, one launch (start us, length us, event | category | flops | bytes accessed | tf_op | source)
XLA Modules:
  0.0 66.5 jit_solution(12638512112402668445)
XLA Ops:
  0.0 1.3 %copy.8.ld_ref = f32[2,1]{1,0:T(2,128)} copy(f32[2,1]{0,1:T(1,128)} %param.12) | data formatting | bytes 16 | tf_op args[5]
  1.3 63.3 %retention.1 = bf16[1,128,2048]{2,1,0:T(8,128)(2,1)} custom-call(bf16[1,128,2048]{2,1,0:T(8,128)(2,1)} %tok_hbm.1, bf16[128,1024]{1,0:T(8,128)(2,1)} %q_hbm.1, bf16[128,1024]{1,0:T(8,128)(2,1)} %k_hbm.1, bf16[128,2048]{1,0:T(8,128)(2,1)} %v_hbm.1, bf16[128,2048]{1,0:T(8,128)(2,1)} %o_hbm.1, f32[2,1]{1,0:T(2,128)} %copy.8.ld_ref, f32[1,128]{1,0:T(1,128)} %constant.2.clone.freq_ref), custom_call_target="tpu_custom_call" | custom-call | tf_op jit(solution)/shard_map/retention/pallas_call | solution.py:502
  64.6 1.9 %copy.10 = bf16[1,128,2048]{2,1,0:T(8,128)(2,1)} copy(bf16[1,128,2048]{2,1,0:T(8,128)(2,1)} %retention.1) | data formatting | bytes 1048576

commit v3 on v2

--- a/solution.py
+++ b/solution.py
@@ -18,6 +18,8 @@
 PAIRS = 2
 EPS = 1e-6
 KV = 768
+PART = 384
+REST = 512
 
 F32 = jnp.float32
 BF16 = jnp.bfloat16
@@ -33,10 +35,10 @@
 
 def kernel(
     tok_hbm, q_hbm, k_hbm, v_hbm, o_hbm, ld_ref, freq_ref, out_ref,
-    tok, wq, wk, wo, own_rate, rates, acc_q, acc_k, cosine, sine, tiles, decay, qr, kr, vb, qs, ks,
+    tok, wq, wk, wo, wz, own_rate, rates, acc_q, acc_k, cosine, sine, tiles, decay, qr, kr, vb, qs, ks,
     ab, states, carried, ret, ns, relay, nb, acc_o,
     local_sem, tok_s, tok_r, wq_s, wq_r, wqd_s, wqd_r, wk_s, wk_r, wkd_s, wkd_r, wo_s, wo_r,
-    wy_s, wy_r, wf_s, wf_r, wod_s, wod_r, own_s, own_r, st_s, st_r, nb_s, nb_r, ld_s, ld_r,
+    wy_s, wy_r, wf_s, wf_r, wod_s, wod_r, own_s, own_r, wz_s, wz_r, wzd_s, wzd_r, st_s, st_r, nb_s, nb_r, ld_s, ld_r,
 ):
     sp = lax.axis_index("sp")
     dp = lax.axis_index("dp")
@@ -80,14 +82,15 @@
         fetched.append(copy)
 
     for part in range(SIDE):
-        fetch(o_hbm.at[:, part * 512:(part + 1) * 512], wo.at[part, dp])
+        fetch(o_hbm.at[:, part * PART:(part + 1) * PART], wo.at[part, dp])
+    fetch(o_hbm.at[:, SIDE * PART:D], wz.at[dp])
     fetch(tok_hbm.at[0], tok.at[x])
     fetch(k_hbm.at[:, pl.ds(pl.multiple_of(x * 256, 256), 256)], wk.at[dp, :, 0:256])
     fetch(v_hbm.at[:, pl.ds(pl.multiple_of(x * 512, 512), 512)], wk.at[dp, :, 256:KV])
     fetch(q_hbm.at[:, pl.ds(pl.multiple_of(x * 256, 256), 256)], wq.at[dp])
 
     sub = lax.broadcasted_iota(jnp.int32, (8, 128), 0)
-    own_rate[...] = jnp.where(sub == 0, ld_ref[0:1, 0:1], ld_ref[1:2, 0:1])
+    own_rate[...] = jnp.where(sub == 0, ld_ref[0:1, 0:1], ld_ref[0:1, 1:2])
 
     barrier = pltpu.get_barrier_semaphore()
     peers = [(lax.rem(sp + o, SIDE * SIDE), dp) for o in range(1, SIDE * SIDE)]
@@ -152,6 +155,9 @@
 
     def q_step(step):
         weight_step(wq, step, wq_s, wq_r, wqd_s, wqd_r)
+
+    def zz_step(step):
+        weight_step(wz, step, wz_s, wz_r, wzd_s, wzd_r)
 
     def share(part, n, index):
         send(part, part, wod_s.at[n, index], wod_r.at[n, index], other_core)
@@ -413,13 +419,21 @@
             normed_all()
         for n in ((0, 1, 2, 3, 4), (5, 6, 7))[stage]:
             take_output(n)
-        for part in range(SIDE):
-            cols = slice(part * 512, (part + 1) * 512)
-            total = jnp.zeros((ROWS, 512), F32) if stage == 0 else acc_o[:, cols]
-            for offset in ((0, 1, 7, 2, 6), (3, 5, 4))[stage]:
-                at = mod(z + offset, RING)
-                lhs = nb[lax.div(at, 2), :, pl.ds(pl.multiple_of(lax.rem(at, 2) * 256, 256), 256)]
-                total = total + matmul(lhs, wo[part, pl.ds(at * 2, 2)].reshape(256, 512))
+            arrive(wz.at[nth_other(n)], wzd_s.at[n], wzd_r.at[n])
+        offsets = ((0, 1, 7, 2, 6), (3, 5, 4))[stage]
+        left_hand, blocks = [], []
+        for offset in offsets:
+            at = mod(z + offset, RING)
+            start = pl.multiple_of(lax.rem(at, 2) * 256, 256)
+            left_hand.append(nb[lax.div(at, 2), :, pl.ds(start, 256)])
+            blocks.append(pl.ds(at * 2, 2))
+        for part in range(SIDE + 1):
+            width = PART if part < SIDE else REST
+            cols = slice(part * PART, part * PART + width)
+            total = jnp.zeros((ROWS, width), F32) if stage == 0 else acc_o[:, cols]
+            for lhs, rows in zip(left_hand, blocks):
+                weight = wo[part, rows] if part < SIDE else wz[rows]
+                total = total + matmul(lhs, weight.reshape(256, width))
             if stage == 0:
                 acc_o[:, cols] = total
             else:
@@ -429,57 +443,62 @@
         with jax.named_scope(name):
             task(*arguments)
 
+    run("K0", k_step, 0)
+    run("Q0", q_step, 0)
+    run("T0", tokens_first)
+    run("LD", send_rates)
+    run("T1", tokens_second)
     run("O0", o_step, 0)
-    run("K0", k_step, 0)
-    run("T0", tokens_first)
+    run("TAB", tables)
+    run("K1", k_step, 1)
     run("O1", o_step, 1)
-    run("TAB", tables)
-    run("Q0", q_step, 0)
-    run("LD", send_rates)
     run("TF", tokens_forward)
-    run("K1", k_step, 1)
-    run("T1", tokens_second)
-    run("SO0", own_output_block)
-    run("DEC", decays)
+    run("Q1", q_step, 1)
+    run("K2", k_step, 2)
     run("O2", o_step, 2)
     run("F1", f_step, 1)
-    run("K2", k_step, 2)
-    run("F2", f_step, 2)
+    run("DEC", decays)
     run("TA", tokens_all)
     run("KA", k_project, 0)
-    run("Q1", q_step, 1)
-    run("G1", g_step, 1)
-    run("QA", q_project, 0)
+    run("KB", k_project, 1)
     run("K3", k_step, 3)
+    run("F2", f_step, 2)
+    run("Q2", q_step, 2)
+    run("Z0", zz_step, 0)
     run("O3", o_step, 3)
-    run("Q2", q_step, 2)
-    run("KB", k_project, 1)
     run("KC", k_project, 2)
     run("K4", k_step, 4)
     run("KD", k_project, 3)
+    run("G2", g_step, 2)
     run("RK", keys_values)
     run("Q3", q_step, 3)
+    run("QA", q_project, 0)
+    run("QB", q_project, 1)
+    run("Z1", zz_step, 1)
+    run("G1", g_step, 1)
+    run("QC", q_project, 2)
     run("Q4", q_step, 4)
-    run("G2", g_step, 2)
-    run("QB", q_project, 1)
-    run("QC", q_project, 2)
     run("O4", o_step, 4)
-    run("F3", f_step, 3)
+    run("SO0", own_output_block)
     run("QD", q_project, 3)
     run("RQ", queries)
+    run("I1", in_block, to_rows[1])
     run("I0", in_block, to_rows[0])
-    run("I1", in_block, to_rows[1])
+    run("Z2", zz_step, 2)
     run("CAR", carry_states)
     run("N0", normed, 0)
+    run("N1", normed, 1)
     run("I2", in_block, to_rows[2])
-    run("N1", normed, 1)
     run("N2", normed, 2)
+    run("F3", f_step, 3)
+    run("I3", in_block, to_rows[3])
     run("F4", f_step, 4)
+    run("N3", normed, 3)
     run("NF", normed_forward)
+    run("Z3", zz_step, 3)
     run("G3", g_step, 3)
-    run("I3", in_block, to_rows[3])
     run("G4", g_step, 4)
-    run("N3", normed, 3)
+    run("Z4", zz_step, 4)
     run("OA", output, 0)
     run("OB", output, 1)
     for copy in sends:
@@ -501,14 +520,15 @@
     dma = pltpu.SemaphoreType.DMA
     return pl.pallas_call(
         kernel,
-        out_shape=jax.ShapeDtypeStruct((1, ROWS, D), BF16),
+        out_shape=pltpu.VMEM((1, ROWS, D), BF16),
         in_specs=[anywhere] * 5 + [vmem] * 2,
         out_specs=vmem,
         scratch_shapes=[
             pltpu.VMEM((SIDE, ROWS, D), BF16),
             pltpu.VMEM((16, 128, 256), BF16),
             pltpu.VMEM((16, 128, KV), BF16),
-            pltpu.VMEM((SIDE, 16, 128, 512), BF16),
+            pltpu.VMEM((SIDE, 16, 128, PART), BF16),
+            pltpu.VMEM((16, 128, REST), BF16),
             pltpu.VMEM((8, 128), F32),
             pltpu.VMEM((SIDE, 8, 128), F32),
             pltpu.VMEM((BLOCK, 256), F32),
@@ -530,12 +550,13 @@
             pltpu.VMEM((2, 64, 512), BF16),
             pltpu.VMEM((SIDE, ROWS, 512), BF16),
             pltpu.VMEM((ROWS, D), F32),
-            dma((8,)), dma((6,)), dma((6,)),
+            dma((9,)), dma((6,)), dma((6,)),
             dma((2, 4)), dma((2, 4)), dma((8,)), dma((8,)),
             dma((2, 4)), dma((2, 4)), dma((8,)), dma((8,)),
             dma((2, 4)), dma((2, 4)),
             dma((8, 2)), dma((8, 2)), dma((8, 2)), dma((8, 2)),
             dma((8, 4)), dma((8, 4)), dma((1,)), dma((1,)),
+            dma((2, 4)), dma((2, 4)), dma((8,)), dma((8,)),
             dma((3,)), dma((3,)), dma((6,)), dma((6,)), dma((4,)), dma((4,)),
         ],
         compiler_params=pltpu.CompilerParams(
@@ -543,7 +564,7 @@
         ),
         name="retention",
     )(
-        tokens, query_weight, key_weight, value_weight, output_weight, log_decay, frequency
+        tokens, query_weight, key_weight, value_weight, output_weight, log_decay.T, frequency
     )
 
 

time: 66.7 us -> 62.8 us (0.942)
  local copies, waits for them, and re-layouts: 3.18 us -> 0.8 us
  Pallas kernels: 63.3 us -> 61.9 us
    unnamed x2 -> x1, local copies, waits for them, and re-layouts: 3.18 us -> 0.8 us
    pallas_call x1, Pallas kernels: 63.3 us -> 61.9 us  [shards(): pl.pallas_call(kernel, out_shape=pltpu.VMEM((1, ROWS, D), BF16), in_specs...]
where the time goes in v3:
time: 62.8 us; the launch traced here: 62.7 us
  Pallas kernels  61.9 us (99%)
  local copies, waits for them, and re-layouts  0.8 us (1%)
    pallas_call x1, Pallas kernels, shards(): pl.pallas_call(kernel, out_shape=pltpu.VMEM((1, ROWS, D), BF16), in_specs...  61.9 us

profile of v3, /device:TPU:1, one launch (start us, length us, event | category | flops | bytes accessed | tf_op | source)
XLA Modules:
  0.0 62.7 jit_solution(6438937123590609303)
XLA Ops:
  0.0 61.9 %retention.1 = bf16[1,128,2048]{2,1,0:T(8,128)(2,1)S(1)} custom-call(bf16[1,128,2048]{2,1,0:T(8,128)(2,1)} %tok_hbm.1, bf16[128,1024]{1,0:T(8,128)(2,1)} %q_hbm.1, bf16[128,1024]{1,0:T(8,128)(2,1)} %k_hbm.1, bf16[128,2048]{1,0:T(8,128)(2,1)} %v_hbm.1, bf16[128,2048]{1,0:T(8,128)(2,1)} %o_hbm.1, f32[1,2]{1,0:T(1,128)} %bitcast.1, f32[1,128]{1,0:T(1,128)} %constant.2.clone.freq_ref), custom_call_target="tpu_custom_call" | custom-call | tf_op jit(solution)/shard_map/retention/pallas_call | solution.py:521
  61.9 0.8 %copy.9 = bf16[1,128,2048]{2,1,0:T(8,128)(2,1)} copy(bf16[1,128,2048]{2,1,0:T(8,128)(2,1)S(1)} %retention.1) | data formatting | bytes 1048576

commit v4 on v3

--- a/solution.py
+++ b/solution.py
@@ -34,8 +34,8 @@
 
 
 def kernel(
-    tok_hbm, q_hbm, k_hbm, v_hbm, o_hbm, ld_ref, freq_ref, out_ref,
-    tok, wq, wk, wo, wz, own_rate, rates, acc_q, acc_k, cosine, sine, tiles, decay, qr, kr, vb, qs, ks,
+    tok_hbm, q_hbm, k_hbm, v_hbm, o_hbm, ld_hbm, freq_hbm, out_ref,
+    tok, wq, wk, wo, wz, ld_ref, freq_ref, own_rate, rates, acc_q, acc_k, cosine, sine, tiles, decay, qr, kr, vb, qs, ks,
     ab, states, carried, ret, ns, relay, nb, acc_o,
     local_sem, tok_s, tok_r, wq_s, wq_r, wqd_s, wqd_r, wk_s, wk_r, wkd_s, wkd_r, wo_s, wo_r,
     wy_s, wy_r, wf_s, wf_r, wod_s, wod_r, own_s, own_r, wz_s, wz_r, wzd_s, wzd_r, st_s, st_r, nb_s, nb_r, ld_s, ld_r,
@@ -81,16 +81,16 @@
         copy.start()
         fetched.append(copy)
 
+    fetch(ld_hbm, ld_ref)
+    fetch(k_hbm.at[:, pl.ds(pl.multiple_of(x * 256, 256), 256)], wk.at[dp, :, 0:256])
+    fetch(v_hbm.at[:, pl.ds(pl.multiple_of(x * 512, 512), 512)], wk.at[dp, :, 256:KV])
+    fetch(tok_hbm.at[0], tok.at[x])
     for part in range(SIDE):
         fetch(o_hbm.at[:, part * PART:(part + 1) * PART], wo.at[part, dp])
+    fetch(q_hbm.at[:, pl.ds(pl.multiple_of(x * 256, 256), 256)], wq.at[dp])
+    fetch(freq_hbm, freq_ref)
     fetch(o_hbm.at[:, SIDE * PART:D], wz.at[dp])
-    fetch(tok_hbm.at[0], tok.at[x])
-    fetch(k_hbm.at[:, pl.ds(pl.multiple_of(x * 256, 256), 256)], wk.at[dp, :, 0:256])
-    fetch(v_hbm.at[:, pl.ds(pl.multiple_of(x * 512, 512), 512)], wk.at[dp, :, 256:KV])
-    fetch(q_hbm.at[:, pl.ds(pl.multiple_of(x * 256, 256), 256)], wq.at[dp])
-
-    sub = lax.broadcasted_iota(jnp.int32, (8, 128), 0)
-    own_rate[...] = jnp.where(sub == 0, ld_ref[0:1, 0:1], ld_ref[0:1, 1:2])
+    needed = {"LD": (0,), "K0": (1, 2), "T0": (3,), "O0": (4, 5, 6, 7), "Q0": (8,), "TAB": (9,), "Z0": (10,)}
 
     barrier = pltpu.get_barrier_semaphore()
     peers = [(lax.rem(sp + o, SIDE * SIDE), dp) for o in range(1, SIDE * SIDE)]
@@ -100,8 +100,6 @@
             barrier, inc=1, device_id=peer, device_id_type=pl.DeviceIdType.MESH
         )
     pl.semaphore_wait(barrier, len(peers))
-    for copy in fetched:
-        copy.wait()
 
     def half(direction):
         return h0 if direction == 0 else h1
@@ -173,7 +171,6 @@
                 part = wo.at[y, nth_block(n)]
                 send(part, part, wy_s.at[n, 0], wy_r.at[n, 0], at_y(above))
                 send(part, part, wy_s.at[n, 1], wy_r.at[n, 1], at_y(below))
-                share(part, n, 0)
 
     def f_step(step):
         for n in blocks_of(step):
@@ -183,8 +180,11 @@
             up, down = wo.at[below, b, h0], wo.at[above, b, h1]
             send(up, up, wf_s.at[n, 0], wf_r.at[n, 0], at_y(above))
             send(down, down, wf_s.at[n, 1], wf_r.at[n, 1], at_y(below))
-            share(wo.at[below, b], n, 1)
-            share(wo.at[above, b], n, 2)
+
+    def d_step(step):
+        for n in blocks_of(step):
+            for index, part in enumerate((y, below, above)):
+                share(wo.at[part, nth_block(n)], n, index)
 
     def g_step(step):
         for n in blocks_of(step):
@@ -225,6 +225,8 @@
         )
 
     def send_rates():
+        sub = lax.broadcasted_iota(jnp.int32, (8, 128), 0)
+        own_rate[...] = jnp.where(sub == 0, ld_ref[0:1, 0:1], ld_ref[0:1, 1:2])
         for to in range(SIDE):
             @pl.when(jnp.logical_or(y != x, y != to))
             def _():
@@ -441,64 +443,70 @@
 
     def run(name, task, *arguments):
         with jax.named_scope(name):
+            for n in needed.get(name, ()):
+                fetched[n].wait()
             task(*arguments)
 
     run("K0", k_step, 0)
-    run("Q0", q_step, 0)
     run("T0", tokens_first)
     run("LD", send_rates)
     run("T1", tokens_second)
     run("O0", o_step, 0)
     run("TAB", tables)
     run("K1", k_step, 1)
+    run("Q0", q_step, 0)
+    run("TF", tokens_forward)
     run("O1", o_step, 1)
-    run("TF", tokens_forward)
+    run("K2", k_step, 2)
     run("Q1", q_step, 1)
-    run("K2", k_step, 2)
     run("O2", o_step, 2)
     run("F1", f_step, 1)
-    run("DEC", decays)
     run("TA", tokens_all)
     run("KA", k_project, 0)
+    run("K3", k_step, 3)
+    run("QA", q_project, 0)
+    run("Q2", q_step, 2)
+    run("SO0", own_output_block)
+    run("Z0", zz_step, 0)
+    run("F2", f_step, 2)
     run("KB", k_project, 1)
-    run("K3", k_step, 3)
-    run("F2", f_step, 2)
-    run("Q2", q_step, 2)
-    run("Z0", zz_step, 0)
+    run("D1", d_step, 1)
     run("O3", o_step, 3)
+    run("QB", q_project, 1)
+    run("G1", g_step, 1)
+    run("K4", k_step, 4)
+    run("DEC", decays)
+    run("D2", d_step, 2)
+    run("G2", g_step, 2)
+    run("Q3", q_step, 3)
     run("KC", k_project, 2)
-    run("K4", k_step, 4)
     run("KD", k_project, 3)
-    run("G2", g_step, 2)
     run("RK", keys_values)
-    run("Q3", q_step, 3)
-    run("QA", q_project, 0)
-    run("QB", q_project, 1)
     run("Z1", zz_step, 1)
-    run("G1", g_step, 1)
+    run("O4", o_step, 4)
+    run("F3", f_step, 3)
     run("QC", q_project, 2)
     run("Q4", q_step, 4)
-    run("O4", o_step, 4)
-    run("SO0", own_output_block)
     run("QD", q_project, 3)
     run("RQ", queries)
-    run("I1", in_block, to_rows[1])
+    run("I2", in_block, to_rows[2])
+    run("Z2", zz_step, 2)
     run("I0", in_block, to_rows[0])
-    run("Z2", zz_step, 2)
     run("CAR", carry_states)
     run("N0", normed, 0)
+    run("I1", in_block, to_rows[1])
     run("N1", normed, 1)
-    run("I2", in_block, to_rows[2])
     run("N2", normed, 2)
-    run("F3", f_step, 3)
+    run("F4", f_step, 4)
     run("I3", in_block, to_rows[3])
-    run("F4", f_step, 4)
-    run("N3", normed, 3)
+    run("D4", d_step, 4)
+    run("D3", d_step, 3)
+    run("Z3", zz_step, 3)
     run("NF", normed_forward)
-    run("Z3", zz_step, 3)
     run("G3", g_step, 3)
     run("G4", g_step, 4)
     run("Z4", zz_step, 4)
+    run("N3", normed, 3)
     run("OA", output, 0)
     run("OB", output, 1)
     for copy in sends:
@@ -521,7 +529,7 @@
     return pl.pallas_call(
         kernel,
         out_shape=pltpu.VMEM((1, ROWS, D), BF16),
-        in_specs=[anywhere] * 5 + [vmem] * 2,
+        in_specs=[anywhere] * 7,
         out_specs=vmem,
         scratch_shapes=[
             pltpu.VMEM((SIDE, ROWS, D), BF16),
@@ -529,6 +537,8 @@
             pltpu.VMEM((16, 128, KV), BF16),
             pltpu.VMEM((SIDE, 16, 128, PART), BF16),
             pltpu.VMEM((16, 128, REST), BF16),
+            pltpu.VMEM((1, 2), F32),
+            pltpu.VMEM((1, 128), F32),
             pltpu.VMEM((8, 128), F32),
             pltpu.VMEM((SIDE, 8, 128), F32),
             pltpu.VMEM((BLOCK, 256), F32),
@@ -550,7 +560,7 @@
             pltpu.VMEM((2, 64, 512), BF16),
             pltpu.VMEM((SIDE, ROWS, 512), BF16),
             pltpu.VMEM((ROWS, D), F32),
-            dma((9,)), dma((6,)), dma((6,)),
+            dma((11,)), dma((6,)), dma((6,)),
             dma((2, 4)), dma((2, 4)), dma((8,)), dma((8,)),
             dma((2, 4)), dma((2, 4)), dma((8,)), dma((8,)),
             dma((2, 4)), dma((2, 4)),

time: 62.8 us -> 60.3 us (0.960)
  Pallas kernels: 61.9 us -> 59.5 us
    pallas_call x1, Pallas kernels: 61.9 us -> 59.5 us  [shards(): pl.pallas_call(kernel, out_shape=pltpu.VMEM((1, ROWS, D), BF16), in_specs...]
where the time goes in v4:
time: 60.3 us
  Pallas kernels  59.5 us (99%)
  local copies, waits for them, and re-layouts  0.8 us (1%)
    pallas_call x1, Pallas kernels, shards(): pl.pallas_call(kernel, out_shape=pltpu.VMEM((1, ROWS, D), BF16), in_specs...  59.5 us

profile of v4, /device:TPU:1, one launch (start us, length us, event | category | flops | bytes accessed | tf_op | source)
XLA Modules:
  0.0 60.3 jit_solution(16356794839711013979)
XLA Ops:
  0.0 59.5 %retention.1 = bf16[1,128,2048]{2,1,0:T(8,128)(2,1)S(1)} custom-call(bf16[1,128,2048]{2,1,0:T(8,128)(2,1)} %tok_hbm.1, bf16[128,1024]{1,0:T(8,128)(2,1)} %q_hbm.1, bf16[128,1024]{1,0:T(8,128)(2,1)} %k_hbm.1, bf16[128,2048]{1,0:T(8,128)(2,1)} %v_hbm.1, bf16[128,2048]{1,0:T(8,128)(2,1)} %o_hbm.1, f32[1,2]{1,0:T(1,128)} %bitcast.1, f32[1,128]{1,0:T(1,128)} %constant.2.clone.freq_hbm), custom_call_target="tpu_custom_call" | custom-call | tf_op jit(solution)/shard_map/retention/pallas_call | solution.py:529
  59.5 0.8 %copy.9 = bf16[1,128,2048]{2,1,0:T(8,128)(2,1)} copy(bf16[1,128,2048]{2,1,0:T(8,128)(2,1)S(1)} %retention.1) | data formatting | bytes 1048576

commit v5 on v4

--- a/solution.py
+++ b/solution.py
@@ -38,7 +38,7 @@
     tok, wq, wk, wo, wz, ld_ref, freq_ref, own_rate, rates, acc_q, acc_k, cosine, sine, tiles, decay, qr, kr, vb, qs, ks,
     ab, states, carried, ret, ns, relay, nb, acc_o,
     local_sem, tok_s, tok_r, wq_s, wq_r, wqd_s, wqd_r, wk_s, wk_r, wkd_s, wkd_r, wo_s, wo_r,
-    wy_s, wy_r, wf_s, wf_r, wod_s, wod_r, own_s, own_r, wz_s, wz_r, wzd_s, wzd_r, st_s, st_r, nb_s, nb_r, ld_s, ld_r,
+    wy_s, wy_r, wf_s, wf_r, wod_s, wod_r, own_s, own_r, wz_s, wz_r, wzd_s, wzd_r, st_s, st_r, nb_s, nb_r, ld_s, ld_r, lr_r,
 ):
     sp = lax.axis_index("sp")
     dp = lax.axis_index("dp")
@@ -81,24 +81,24 @@
         copy.start()
         fetched.append(copy)
 
-    fetch(ld_hbm, ld_ref)
     fetch(k_hbm.at[:, pl.ds(pl.multiple_of(x * 256, 256), 256)], wk.at[dp, :, 0:256])
     fetch(v_hbm.at[:, pl.ds(pl.multiple_of(x * 512, 512), 512)], wk.at[dp, :, 256:KV])
+
+    barrier = pltpu.get_barrier_semaphore()
+    peers = [at_z(mod(z + 1, RING)), at_z(mod(z - 1, RING)), other_core]
+    peers += [at_x(to) for to in (right, left, across)] + [at_y(to) for to in (above, below, facing)]
+    for peer in peers:
+        pl.semaphore_signal(
+            barrier, inc=1, device_id=peer, device_id_type=pl.DeviceIdType.MESH
+        )
     fetch(tok_hbm.at[0], tok.at[x])
+    fetch(ld_hbm, ld_ref)
     for part in range(SIDE):
         fetch(o_hbm.at[:, part * PART:(part + 1) * PART], wo.at[part, dp])
     fetch(q_hbm.at[:, pl.ds(pl.multiple_of(x * 256, 256), 256)], wq.at[dp])
     fetch(freq_hbm, freq_ref)
     fetch(o_hbm.at[:, SIDE * PART:D], wz.at[dp])
-    needed = {"LD": (0,), "K0": (1, 2), "T0": (3,), "O0": (4, 5, 6, 7), "Q0": (8,), "TAB": (9,), "Z0": (10,)}
-
-    barrier = pltpu.get_barrier_semaphore()
-    peers = [(lax.rem(sp + o, SIDE * SIDE), dp) for o in range(1, SIDE * SIDE)]
-    peers += [at_z(mod(z + 1, RING)), at_z(mod(z - 1, RING)), other_core]
-    for peer in peers:
-        pl.semaphore_signal(
-            barrier, inc=1, device_id=peer, device_id_type=pl.DeviceIdType.MESH
-        )
+    needed = {"K0": (0, 1), "T0": (2,), "LD": (3,), "O0": (4, 5, 6, 7), "Q0": (8,), "TAB": (9,), "Z0": (10,)}
     pl.semaphore_wait(barrier, len(peers))
 
     def half(direction):
@@ -218,23 +218,37 @@
         arrive(tok.at[right, h1], tok_s.at[1], tok_r.at[1])
         send(tok.at[right, h1], tok.at[right, h1], tok_s.at[5], tok_r.at[5], at_x(left))
 
-    def rate_copy(to):
+    def rate_copy():
         return pltpu.make_async_remote_copy(
-            src_ref=own_rate, dst_ref=rates.at[x], send_sem=ld_s.at[to], recv_sem=ld_r.at[x],
-            device_id=(to * SIDE + y, dp), device_id_type=pl.DeviceIdType.MESH,
+            src_ref=own_rate, dst_ref=rates.at[x], send_sem=ld_s.at[0], recv_sem=ld_r.at[x],
+            device_id=at_x(y), device_id_type=pl.DeviceIdType.MESH,
+        )
+
+    def rates_copy(n, to):
+        return pltpu.make_async_remote_copy(
+            src_ref=rates, dst_ref=rates, send_sem=ld_s.at[n], recv_sem=lr_r.at[0],
+            device_id=at_y(to), device_id_type=pl.DeviceIdType.MESH,
         )
 
     def send_rates():
         sub = lax.broadcasted_iota(jnp.int32, (8, 128), 0)
         own_rate[...] = jnp.where(sub == 0, ld_ref[0:1, 0:1], ld_ref[0:1, 1:2])
-        for to in range(SIDE):
-            @pl.when(jnp.logical_or(y != x, y != to))
-            def _():
-                rate_copy(to).start()
-
-            @pl.when(jnp.logical_and(y == x, y == to))
-            def _():
-                pltpu.make_async_copy(own_rate, rates.at[x], ld_r.at[x]).start()
+
+        @pl.when(x != y)
+        def _():
+            rate_copy().start()
+
+        @pl.when(x == y)
+        def _():
+            pltpu.make_async_copy(own_rate, rates.at[x], ld_r.at[x]).start()
+
+    def forward_rates():
+        @pl.when(x == y)
+        def _():
+            for j in range(SIDE):
+                arrive(rates.at[j], ld_s.at[0], ld_r.at[j])
+            for n, to in enumerate((above, below, facing)):
+                rates_copy(n + 1, to).start()
 
     lane = lax.broadcasted_iota(jnp.int32, (1, 128), 1)
     low = lax.rem(lane, 64) < 32
@@ -249,8 +263,9 @@
             sine[rows, :] = jnp.where(low, -turned, turned)
 
     def decays():
-        for j in range(SIDE):
-            arrive(rates.at[j], ld_s.at[j], ld_r.at[j])
+        @pl.when(x != y)
+        def _():
+            arrive(rates, ld_s.at[0], lr_r.at[0])
 
         def decay_tiles(h, carry):
             a, b = rates[h, 0:1, :], rates[h, 1:2, :]
@@ -448,13 +463,14 @@
             task(*arguments)
 
     run("K0", k_step, 0)
+    run("LD", send_rates)
     run("T0", tokens_first)
-    run("LD", send_rates)
     run("T1", tokens_second)
     run("O0", o_step, 0)
     run("TAB", tables)
     run("K1", k_step, 1)
     run("Q0", q_step, 0)
+    run("LF", forward_rates)
     run("TF", tokens_forward)
     run("O1", o_step, 1)
     run("K2", k_step, 2)
@@ -511,10 +527,14 @@
     run("OB", output, 1)
     for copy in sends:
         copy.wait_send()
-    for to in range(SIDE):
-        @pl.when(jnp.logical_or(y != x, y != to))
-        def _():
-            rate_copy(to).wait_send()
+    @pl.when(x != y)
+    def _():
+        rate_copy().wait_send()
+
+    @pl.when(x == y)
+    def _():
+        for n, to in enumerate((above, below, facing)):
+            rates_copy(n + 1, to).wait_send()
 
 
 def shards(tokens, query_weight, key_weight, value_weight, output_weight, log_decay):
@@ -567,7 +587,7 @@
             dma((8, 2)), dma((8, 2)), dma((8, 2)), dma((8, 2)),
             dma((8, 4)), dma((8, 4)), dma((1,)), dma((1,)),
             dma((2, 4)), dma((2, 4)), dma((8,)), dma((8,)),
-            dma((3,)), dma((3,)), dma((6,)), dma((6,)), dma((4,)), dma((4,)),
+            dma((3,)), dma((3,)), dma((6,)), dma((6,)), dma((4,)), dma((4,)), dma((1,)),
         ],
         compiler_params=pltpu.CompilerParams(
             collective_id=0, has_side_effects=True, vmem_limit_bytes=60 * 1024 * 1024

time: 60.3 us -> 58.9 us (0.977)
  Pallas kernels: 59.5 us -> 58 us
    pallas_call x1, Pallas kernels: 59.5 us -> 58 us  [shards(): pl.pallas_call(kernel, out_shape=pltpu.VMEM((1, ROWS, D), BF16), in_specs...]
where the time goes in v5:
time: 58.9 us; the launch traced here: 58.8 us
  Pallas kernels  58 us (98%)
  local copies, waits for them, and re-layouts  0.8 us (1%)
    pallas_call x1, Pallas kernels, shards(): pl.pallas_call(kernel, out_shape=pltpu.VMEM((1, ROWS, D), BF16), in_specs...  58 us

profile of v5, /device:TPU:1, one launch (start us, length us, event | category | flops | bytes accessed | tf_op | source)
XLA Modules:
  0.0 58.8 jit_solution(11024945637824486115)
XLA Ops:
  0.0 58.0 %retention.1 = bf16[1,128,2048]{2,1,0:T(8,128)(2,1)S(1)} custom-call(bf16[1,128,2048]{2,1,0:T(8,128)(2,1)} %tok_hbm.1, bf16[128,1024]{1,0:T(8,128)(2,1)} %q_hbm.1, bf16[128,1024]{1,0:T(8,128)(2,1)} %k_hbm.1, bf16[128,2048]{1,0:T(8,128)(2,1)} %v_hbm.1, bf16[128,2048]{1,0:T(8,128)(2,1)} %o_hbm.1, f32[1,2]{1,0:T(1,128)} %bitcast.1, f32[1,128]{1,0:T(1,128)} %constant.2.clone.freq_hbm), custom_call_target="tpu_custom_call" | custom-call | tf_op jit(solution)/shard_map/retention/pallas_call | solution.py:549
  58.0 0.8 %copy.9 = bf16[1,128,2048]{2,1,0:T(8,128)(2,1)} copy(bf16[1,128,2048]{2,1,0:T(8,128)(2,1)S(1)} %retention.1) | data formatting | bytes 1048576

commit v6 on v5

--- a/solution.py
+++ b/solution.py
@@ -38,7 +38,7 @@
     tok, wq, wk, wo, wz, ld_ref, freq_ref, own_rate, rates, acc_q, acc_k, cosine, sine, tiles, decay, qr, kr, vb, qs, ks,
     ab, states, carried, ret, ns, relay, nb, acc_o,
     local_sem, tok_s, tok_r, wq_s, wq_r, wqd_s, wqd_r, wk_s, wk_r, wkd_s, wkd_r, wo_s, wo_r,
-    wy_s, wy_r, wf_s, wf_r, wod_s, wod_r, own_s, own_r, wz_s, wz_r, wzd_s, wzd_r, st_s, st_r, nb_s, nb_r, ld_s, ld_r, lr_r,
+    wy_s, wy_r, wf_s, wf_r, wod_s, wod_r, wz_s, wz_r, wzd_s, wzd_r, st_s, st_r, nb_s, nb_r, ld_s, ld_r, lr_r,
 ):
     sp = lax.axis_index("sp")
     dp = lax.axis_index("dp")
@@ -58,15 +58,12 @@
         return (sp, to * 2 + c)
 
     other_core = (sp, z * 2 + (1 - c))
-    sends = []
-
     def send(src, dst, send_sem, recv_sem, to):
         copy = pltpu.make_async_remote_copy(
             src_ref=src, dst_ref=dst, send_sem=send_sem, recv_sem=recv_sem,
             device_id=to, device_id_type=pl.DeviceIdType.MESH,
         )
         copy.start()
-        sends.append(copy)
 
     def arrive(dst, send_sem, recv_sem):
         pltpu.make_async_remote_copy(
@@ -74,15 +71,20 @@
             device_id=other_core, device_id_type=pl.DeviceIdType.MESH,
         ).wait_recv()
 
-    fetched = []
-
-    def fetch(src, dst):
-        copy = pltpu.make_async_copy(src, dst, local_sem.at[len(fetched)])
-        copy.start()
-        fetched.append(copy)
-
-    fetch(k_hbm.at[:, pl.ds(pl.multiple_of(x * 256, 256), 256)], wk.at[dp, :, 0:256])
-    fetch(v_hbm.at[:, pl.ds(pl.multiple_of(x * 512, 512), 512)], wk.at[dp, :, 256:KV])
+    def fetch(src, dst, n):
+        pltpu.make_async_copy(src, dst, local_sem.at[n]).start()
+
+    def fetched(name):
+        if name in groups:
+            n, ref = groups[name]
+            pltpu.make_async_copy(ref, ref, local_sem.at[n]).wait()
+
+    groups = {
+        "K0": (0, wk.at[dp]), "T0": (1, tok.at[x]), "LD": (2, ld_ref), "O0": (3, wo.at[:, dp]),
+        "Q0": (4, wq.at[dp]), "TAB": (5, freq_ref), "Z0": (6, wz.at[dp]),
+    }
+    fetch(k_hbm.at[:, pl.ds(pl.multiple_of(x * 256, 256), 256)], wk.at[dp, :, 0:256], 0)
+    fetch(v_hbm.at[:, pl.ds(pl.multiple_of(x * 512, 512), 512)], wk.at[dp, :, 256:KV], 0)
 
     barrier = pltpu.get_barrier_semaphore()
     peers = [at_z(mod(z + 1, RING)), at_z(mod(z - 1, RING)), other_core]
@@ -91,14 +93,13 @@
         pl.semaphore_signal(
             barrier, inc=1, device_id=peer, device_id_type=pl.DeviceIdType.MESH
         )
-    fetch(tok_hbm.at[0], tok.at[x])
-    fetch(ld_hbm, ld_ref)
+    fetch(tok_hbm.at[0], tok.at[x], 1)
+    fetch(ld_hbm, ld_ref, 2)
     for part in range(SIDE):
-        fetch(o_hbm.at[:, part * PART:(part + 1) * PART], wo.at[part, dp])
-    fetch(q_hbm.at[:, pl.ds(pl.multiple_of(x * 256, 256), 256)], wq.at[dp])
-    fetch(freq_hbm, freq_ref)
-    fetch(o_hbm.at[:, SIDE * PART:D], wz.at[dp])
-    needed = {"K0": (0, 1), "T0": (2,), "LD": (3,), "O0": (4, 5, 6, 7), "Q0": (8,), "TAB": (9,), "Z0": (10,)}
+        fetch(o_hbm.at[:, part * PART:(part + 1) * PART], wo.at[part, dp], 3)
+    fetch(q_hbm.at[:, pl.ds(pl.multiple_of(x * 256, 256), 256)], wq.at[dp], 4)
+    fetch(freq_hbm, freq_ref, 5)
+    fetch(o_hbm.at[:, SIDE * PART:D], wz.at[dp], 6)
     pl.semaphore_wait(barrier, len(peers))
 
     def half(direction):
@@ -123,30 +124,27 @@
     def blocks_of(step):
         return (0,) if step == 0 else (2 * step - 1, 2 * step) if step < 4 else (7,)
 
-    def ring_wait(view, step, s_sem, r_sem):
+    def ring_wait(span, step, s_sem, r_sem):
         if step > 0:
-            for d in range(2):
-                b = z_block(d, step)
-                arrive(
-                    view(b) if step < 4 else view(b, half(d)), s_sem.at[d, step - 1], r_sem.at[d, step - 1]
-                )
+            arrive(span(2 if step < 4 else 1), s_sem.at[0], r_sem.at[step - 1])
 
     def ring_send(view, step, s_sem, r_sem):
         if step < 4:
             for d in range(2):
                 b = z_block(d, step)
                 part = view(b) if step < 3 else view(b, half(d))
-                send(part, part, s_sem.at[d, step], r_sem.at[d, step], at_z(z_next(d)))
+                send(part, part, s_sem.at[0], r_sem.at[step], at_z(z_next(d)))
 
     def weight_step(ref, step, s_sem, r_sem, d_s, d_r):
         def view(b, rows=None):
             return ref.at[b] if rows is None else ref.at[b, rows]
 
-        ring_wait(view, step, s_sem, r_sem)
+        ring_wait(lambda count: ref.at[pl.ds(0, count)], step, s_sem, r_sem)
         ring_send(view, step, s_sem, r_sem)
         for n in blocks_of(step):
             b = nth_block(n)
-            send(ref.at[b], ref.at[b], d_s.at[n], d_r.at[n], other_core)
+            group = n // 5 if ref is wz else max(n - 1, 0) // 2
+            send(ref.at[b], ref.at[b], d_s.at[0], d_r.at[group], other_core)
 
     def k_step(step):
         weight_step(wk, step, wk_s, wk_r, wkd_s, wkd_r)
@@ -157,70 +155,60 @@
     def zz_step(step):
         weight_step(wz, step, wz_s, wz_r, wzd_s, wzd_r)
 
-    def share(part, n, index):
-        send(part, part, wod_s.at[n, index], wod_r.at[n, index], other_core)
+    def share(part, n):
+        send(part, part, wod_s.at[0], wod_r.at[n // 5], other_core)
 
     def o_step(step):
         def view(b, rows=None):
             return wo.at[y, b] if rows is None else wo.at[y, b, rows]
 
-        ring_wait(view, step, wo_s, wo_r)
+        ring_wait(lambda count: wo.at[0, pl.ds(0, count)], step, wo_s, wo_r)
         ring_send(view, step, wo_s, wo_r)
         if step > 0:
             for n in blocks_of(step):
                 part = wo.at[y, nth_block(n)]
-                send(part, part, wy_s.at[n, 0], wy_r.at[n, 0], at_y(above))
-                send(part, part, wy_s.at[n, 1], wy_r.at[n, 1], at_y(below))
+                send(part, part, wy_s.at[0], wy_r.at[step - 1], at_y(above))
+                send(part, part, wy_s.at[0], wy_r.at[step - 1], at_y(below))
 
     def f_step(step):
-        for n in blocks_of(step):
+        blocks = blocks_of(step)
+        arrive(wo.at[0, pl.ds(0, 2 * len(blocks))], wy_s.at[0], wy_r.at[step - 1])
+        for n in blocks:
             b = nth_block(n)
-            arrive(wo.at[below, b], wy_s.at[n, 0], wy_r.at[n, 0])
-            arrive(wo.at[above, b], wy_s.at[n, 1], wy_r.at[n, 1])
             up, down = wo.at[below, b, h0], wo.at[above, b, h1]
-            send(up, up, wf_s.at[n, 0], wf_r.at[n, 0], at_y(above))
-            send(down, down, wf_s.at[n, 1], wf_r.at[n, 1], at_y(below))
+            send(up, up, wf_s.at[0], wf_r.at[step - 1], at_y(above))
+            send(down, down, wf_s.at[0], wf_r.at[step - 1], at_y(below))
 
     def d_step(step):
         for n in blocks_of(step):
-            for index, part in enumerate((y, below, above)):
-                share(wo.at[part, nth_block(n)], n, index)
+            for part in (y, below, above):
+                share(wo.at[part, nth_block(n)], n)
 
     def g_step(step):
-        for n in blocks_of(step):
-            b = nth_block(n)
-            arrive(wo.at[facing, b, h0], wf_s.at[n, 0], wf_r.at[n, 0])
-            arrive(wo.at[facing, b, h1], wf_s.at[n, 1], wf_r.at[n, 1])
-            share(wo.at[facing, b], n, 3)
+        blocks = blocks_of(step)
+        arrive(wo.at[0, pl.ds(0, len(blocks))], wf_s.at[0], wf_r.at[step - 1])
+        for n in blocks:
+            share(wo.at[facing, nth_block(n)], n)
 
     def own_output_block():
-        send(wo.at[:, dp], wo.at[:, dp], own_s.at[0], own_r.at[0], other_core)
-
-    def take_output(n):
-        b = nth_other(n)
-        if n == 0:
-            arrive(wo.at[:, b], own_s.at[0], own_r.at[0])
-        else:
-            for index, part in enumerate((y, below, above, facing)):
-                arrive(wo.at[part, b], wod_s.at[n, index], wod_r.at[n, index])
+        send(wo.at[:, dp], wo.at[:, dp], wod_s.at[0], wod_r.at[0], other_core)
 
     def tokens_first():
         send(tok.at[x, h0], tok.at[x, h0], tok_s.at[0], tok_r.at[0], at_x(right))
-        send(tok.at[x, h1], tok.at[x, h1], tok_s.at[1], tok_r.at[1], at_x(left))
+        send(tok.at[x, h1], tok.at[x, h1], tok_s.at[0], tok_r.at[0], at_x(left))
 
     def tokens_second():
-        send(tok.at[x, h1], tok.at[x, h1], tok_s.at[2], tok_r.at[2], at_x(right))
-        send(tok.at[x, h0], tok.at[x, h0], tok_s.at[3], tok_r.at[3], at_x(left))
+        send(tok.at[x, h1], tok.at[x, h1], tok_s.at[0], tok_r.at[1], at_x(right))
+        send(tok.at[x, h0], tok.at[x, h0], tok_s.at[0], tok_r.at[1], at_x(left))
 
     def tokens_forward():
-        arrive(tok.at[left, h0], tok_s.at[0], tok_r.at[0])
-        send(tok.at[left, h0], tok.at[left, h0], tok_s.at[4], tok_r.at[4], at_x(right))
-        arrive(tok.at[right, h1], tok_s.at[1], tok_r.at[1])
-        send(tok.at[right, h1], tok.at[right, h1], tok_s.at[5], tok_r.at[5], at_x(left))
+        arrive(tok.at[0], tok_s.at[0], tok_r.at[0])
+        send(tok.at[left, h0], tok.at[left, h0], tok_s.at[0], tok_r.at[1], at_x(right))
+        send(tok.at[right, h1], tok.at[right, h1], tok_s.at[0], tok_r.at[1], at_x(left))
 
     def rate_copy():
         return pltpu.make_async_remote_copy(
-            src_ref=own_rate, dst_ref=rates.at[x], send_sem=ld_s.at[0], recv_sem=ld_r.at[x],
+            src_ref=own_rate, dst_ref=rates.at[x], send_sem=ld_s.at[0], recv_sem=ld_r.at[0],
             device_id=at_x(y), device_id_type=pl.DeviceIdType.MESH,
         )
 
@@ -240,13 +228,12 @@
 
         @pl.when(x == y)
         def _():
-            pltpu.make_async_copy(own_rate, rates.at[x], ld_r.at[x]).start()
+            pltpu.make_async_copy(own_rate, rates.at[x], ld_r.at[0]).start()
 
     def forward_rates():
         @pl.when(x == y)
         def _():
-            for j in range(SIDE):
-                arrive(rates.at[j], ld_s.at[0], ld_r.at[j])
+            arrive(rates, ld_s.at[0], ld_r.at[0])
             for n, to in enumerate((above, below, facing)):
                 rates_copy(n + 1, to).start()
 
@@ -294,10 +281,7 @@
         lax.fori_loop(0, PAIRS, decay_rows, 0)
 
     def tokens_all():
-        arrive(tok.at[left, h1], tok_s.at[2], tok_r.at[2])
-        arrive(tok.at[right, h0], tok_s.at[3], tok_r.at[3])
-        arrive(tok.at[across, h0], tok_s.at[4], tok_r.at[4])
-        arrive(tok.at[across, h1], tok_s.at[5], tok_r.at[5])
+        arrive(tok.at[pl.ds(0, 2)], tok_s.at[0], tok_r.at[1])
 
     def project(ref, acc, width, offset, fresh):
         at = mod(z + offset, RING)
@@ -321,8 +305,7 @@
         k_or_q(stage, wq, acc_q, 256, wqd_s, wqd_r)
 
     def k_or_q(stage, ref, acc, width, d_s, d_r):
-        for n in ((0, 1, 2), (3, 4), (5, 6), (7,))[stage]:
-            arrive(ref.at[nth_other(n)], d_s.at[n], d_r.at[n])
+        arrive(ref.at[pl.ds(0, (3, 2, 2, 1)[stage])], d_s.at[0], d_r.at[stage])
         if stage == 0:
             project(ref, acc, width, 0, True)
             project_many(ref, acc, width, 1, 2, 6)
@@ -354,8 +337,8 @@
             for d in range(2):
                 square = both[d * 128:(d + 1) * 128]
                 ab[d, p] = jnp.where(row_low, square[:, :128], square[:, 128:]).astype(BF16)
-        for n, to in ((2, facing), (0, above), (1, below)):
-            send(ab.at[jnp.where(to > y, 0, 1)], states.at[y], st_s.at[n], st_r.at[n], at_y(to))
+        for to in (facing, above, below):
+            send(ab.at[jnp.where(to > y, 0, 1)], states.at[y], st_s.at[0], st_r.at[0], at_y(to))
 
     def queries():
         for p in range(PAIRS):
@@ -377,9 +360,7 @@
             ret[r, :, h * 128:(h + 1) * 128] = matmul(scores, vb[h])
 
     def carry_states():
-        arrive(states.at[below], st_s.at[0], st_r.at[0])
-        arrive(states.at[above], st_s.at[1], st_r.at[1])
-        arrive(states.at[facing], st_s.at[2], st_r.at[2])
+        arrive(states.at[pl.ds(0, 3)], st_s.at[0], st_r.at[0])
         for p in range(PAIRS):
             for d in range(2):
                 rate = jnp.where(row_low, rates[2 * p, d:d + 1, 0:1], rates[2 * p + 1, d:d + 1, 0:1])
@@ -415,28 +396,24 @@
         finish_rows(r, ns.at[n])
         if n == 0:
             send(ns.at[0, h0], relay.at[0], nb_s.at[0], nb_r.at[0], at_x(right))
-            send(ns.at[0, h1], relay.at[1], nb_s.at[1], nb_r.at[1], at_x(left))
+            send(ns.at[0, h1], relay.at[1], nb_s.at[0], nb_r.at[0], at_x(left))
         else:
-            send(ns.at[n], nb.at[x], nb_s.at[n + 1], nb_r.at[n + 1], at_x(r))
+            send(ns.at[n], nb.at[x], nb_s.at[0], nb_r.at[1], at_x(r))
 
     def normed_forward():
-        arrive(relay.at[0], nb_s.at[0], nb_r.at[0])
-        send(relay.at[0], nb.at[left, h0], nb_s.at[4], nb_r.at[4], at_x(right))
-        arrive(relay.at[1], nb_s.at[1], nb_r.at[1])
-        send(relay.at[1], nb.at[right, h1], nb_s.at[5], nb_r.at[5], at_x(left))
+        arrive(relay, nb_s.at[0], nb_r.at[0])
+        send(relay.at[0], nb.at[left, h0], nb_s.at[0], nb_r.at[1], at_x(right))
+        send(relay.at[1], nb.at[right, h1], nb_s.at[0], nb_r.at[1], at_x(left))
 
     def normed_all():
-        arrive(nb.at[right], nb_s.at[2], nb_r.at[2])
-        arrive(nb.at[left], nb_s.at[3], nb_r.at[3])
-        arrive(nb.at[across, h0], nb_s.at[4], nb_r.at[4])
-        arrive(nb.at[across, h1], nb_s.at[5], nb_r.at[5])
+        arrive(nb.at[pl.ds(0, 3)], nb_s.at[0], nb_r.at[1])
 
     def output(stage):
         if stage == 0:
             normed_all()
-        for n in ((0, 1, 2, 3, 4), (5, 6, 7))[stage]:
-            take_output(n)
-            arrive(wz.at[nth_other(n)], wzd_s.at[n], wzd_r.at[n])
+        count = (5, 3)[stage]
+        arrive(wo.at[:, pl.ds(0, count)], wod_s.at[0], wod_r.at[stage])
+        arrive(wz.at[pl.ds(0, count)], wzd_s.at[0], wzd_r.at[stage])
         offsets = ((0, 1, 7, 2, 6), (3, 5, 4))[stage]
         left_hand, blocks = [], []
         for offset in offsets:
@@ -458,8 +435,7 @@
 
     def run(name, task, *arguments):
         with jax.named_scope(name):
-            for n in needed.get(name, ()):
-                fetched[n].wait()
+            fetched(name)
             task(*arguments)
 
     run("K0", k_step, 0)
@@ -525,8 +501,17 @@
     run("N3", normed, 3)
     run("OA", output, 0)
     run("OB", output, 1)
-    for copy in sends:
-        copy.wait_send()
+    for ref, sem in (
+        (tok.at[pl.ds(0, 3)], tok_s), (wq.at[pl.ds(0, 7)], wq_s), (wk.at[pl.ds(0, 7)], wk_s),
+        (wz.at[pl.ds(0, 7)], wz_s), (wo.at[0, pl.ds(0, 7)], wo_s), (wq.at[pl.ds(0, 8)], wqd_s),
+        (wk.at[pl.ds(0, 8)], wkd_s), (wz.at[pl.ds(0, 8)], wzd_s), (wo.at[:, pl.ds(0, 8)], wod_s),
+        (wo.at[0, pl.ds(0, 14)], wy_s), (wo.at[0, pl.ds(0, 7)], wf_s),
+        (states.at[pl.ds(0, 3)], st_s), (nb, nb_s),
+    ):
+        pltpu.make_async_remote_copy(
+            src_ref=ref, dst_ref=ref, send_sem=sem.at[0], recv_sem=lr_r.at[0],
+            device_id=other_core, device_id_type=pl.DeviceIdType.MESH,
+        ).wait_send()
     @pl.when(x != y)
     def _():
         rate_copy().wait_send()
@@ -580,14 +565,14 @@
             pltpu.VMEM((2, 64, 512), BF16),
             pltpu.VMEM((SIDE, ROWS, 512), BF16),
             pltpu.VMEM((ROWS, D), F32),
-            dma((11,)), dma((6,)), dma((6,)),
-            dma((2, 4)), dma((2, 4)), dma((8,)), dma((8,)),
-            dma((2, 4)), dma((2, 4)), dma((8,)), dma((8,)),
-            dma((2, 4)), dma((2, 4)),
-            dma((8, 2)), dma((8, 2)), dma((8, 2)), dma((8, 2)),
-            dma((8, 4)), dma((8, 4)), dma((1,)), dma((1,)),
-            dma((2, 4)), dma((2, 4)), dma((8,)), dma((8,)),
-            dma((3,)), dma((3,)), dma((6,)), dma((6,)), dma((4,)), dma((4,)), dma((1,)),
+            dma((7,)), dma((1,)), dma((2,)),
+            dma((1,)), dma((4,)), dma((1,)), dma((4,)),
+            dma((1,)), dma((4,)), dma((1,)), dma((4,)),
+            dma((1,)), dma((4,)),
+            dma((1,)), dma((4,)), dma((1,)), dma((4,)),
+            dma((1,)), dma((2,)),
+            dma((1,)), dma((4,)), dma((1,)), dma((2,)),
+            dma((1,)), dma((1,)), dma((1,)), dma((2,)), dma((4,)), dma((1,)), dma((1,)),
         ],
         compiler_params=pltpu.CompilerParams(
             collective_id=0, has_side_effects=True, vmem_limit_bytes=60 * 1024 * 1024

time: 58.9 us -> 56.7 us (0.963)
  Pallas kernels: 58 us -> 55.8 us
    pallas_call x1, Pallas kernels: 58 us -> 55.8 us  [shards(): pl.pallas_call(kernel, out_shape=pltpu.VMEM((1, ROWS, D), BF16), in_specs...]
where the time goes in v6:
time: 56.7 us; the launch traced here: 56.6 us
  Pallas kernels  55.8 us (98%)
  local copies, waits for them, and re-layouts  0.8 us (1%)
    pallas_call x1, Pallas kernels, shards(): pl.pallas_call(kernel, out_shape=pltpu.VMEM((1, ROWS, D), BF16), in_specs...  55.8 us

profile of v6, /device:TPU:1, one launch (start us, length us, event | category | flops | bytes accessed | tf_op | source)
XLA Modules:
  0.0 56.6 jit_solution(14639707584998599616)
XLA Ops:
  0.0 55.8 %retention.1 = bf16[1,128,2048]{2,1,0:T(8,128)(2,1)S(1)} custom-call(bf16[1,128,2048]{2,1,0:T(8,128)(2,1)} %tok_hbm.1, bf16[128,1024]{1,0:T(8,128)(2,1)} %q_hbm.1, bf16[128,1024]{1,0:T(8,128)(2,1)} %k_hbm.1, bf16[128,2048]{1,0:T(8,128)(2,1)} %v_hbm.1, bf16[128,2048]{1,0:T(8,128)(2,1)} %o_hbm.1, f32[1,2]{1,0:T(1,128)} %bitcast.1, f32[1,128]{1,0:T(1,128)} %constant.2.clone.freq_hbm), custom_call_target="tpu_custom_call" | custom-call | tf_op jit(solution)/shard_map/retention/pallas_call | solution.py:534
  55.8 0.8 %copy.9 = bf16[1,128,2048]{2,1,0:T(8,128)(2,1)} copy(bf16[1,128,2048]{2,1,0:T(8,128)(2,1)S(1)} %retention.1) | data formatting | bytes 1048576

commit v7 on v6

--- a/solution.py
+++ b/solution.py
@@ -443,14 +443,15 @@
     run("T0", tokens_first)
     run("T1", tokens_second)
     run("O0", o_step, 0)
+    run("K1", k_step, 1)
     run("TAB", tables)
-    run("K1", k_step, 1)
     run("Q0", q_step, 0)
     run("LF", forward_rates)
     run("TF", tokens_forward)
     run("O1", o_step, 1)
     run("K2", k_step, 2)
     run("Q1", q_step, 1)
+    run("DEC", decays)
     run("O2", o_step, 2)
     run("F1", f_step, 1)
     run("TA", tokens_all)
@@ -467,7 +468,6 @@
     run("QB", q_project, 1)
     run("G1", g_step, 1)
     run("K4", k_step, 4)
-    run("DEC", decays)
     run("D2", d_step, 2)
     run("G2", g_step, 2)
     run("Q3", q_step, 3)
@@ -481,14 +481,14 @@
     run("Q4", q_step, 4)
     run("QD", q_project, 3)
     run("RQ", queries)
+    run("I0", in_block, to_rows[0])
+    run("Z2", zz_step, 2)
     run("I2", in_block, to_rows[2])
-    run("Z2", zz_step, 2)
-    run("I0", in_block, to_rows[0])
     run("CAR", carry_states)
     run("N0", normed, 0)
+    run("N2", normed, 2)
     run("I1", in_block, to_rows[1])
     run("N1", normed, 1)
-    run("N2", normed, 2)
     run("F4", f_step, 4)
     run("I3", in_block, to_rows[3])
     run("D4", d_step, 4)
@@ -497,8 +497,8 @@
     run("NF", normed_forward)
     run("G3", g_step, 3)
     run("G4", g_step, 4)
+    run("N3", normed, 3)
     run("Z4", zz_step, 4)
-    run("N3", normed, 3)
     run("OA", output, 0)
     run("OB", output, 1)
     for ref, sem in (

time: 56.7 us -> 56.4 us (level)
  no operation moved by 1% of the time
where the time goes in v7:
time: 56.4 us; the launch traced here: 56.3 us
  Pallas kernels  55.5 us (98%)
  local copies, waits for them, and re-layouts  0.8 us (1%)
    pallas_call x1, Pallas kernels, shards(): pl.pallas_call(kernel, out_shape=pltpu.VMEM((1, ROWS, D), BF16), in_specs...  55.5 us

profile of v7, /device:TPU:1, one launch (start us, length us, event | category | flops | bytes accessed | tf_op | source)
XLA Modules:
  0.0 56.3 jit_solution(6762781275103007207)
XLA Ops:
  0.0 55.5 %retention.1 = bf16[1,128,2048]{2,1,0:T(8,128)(2,1)S(1)} custom-call(bf16[1,128,2048]{2,1,0:T(8,128)(2,1)} %tok_hbm.1, bf16[128,1024]{1,0:T(8,128)(2,1)} %q_hbm.1, bf16[128,1024]{1,0:T(8,128)(2,1)} %k_hbm.1, bf16[128,2048]{1,0:T(8,128)(2,1)} %v_hbm.1, bf16[128,2048]{1,0:T(8,128)(2,1)} %o_hbm.1, f32[1,2]{1,0:T(1,128)} %bitcast.1, f32[1,128]{1,0:T(1,128)} %constant.2.clone.freq_hbm), custom_call_target="tpu_custom_call" | custom-call | tf_op jit(solution)/shard_map/retention/pallas_call | solution.py:534
  55.5 0.8 %copy.9 = bf16[1,128,2048]{2,1,0:T(8,128)(2,1)} copy(bf16[1,128,2048]{2,1,0:T(8,128)(2,1)S(1)} %retention.1) | data formatting | bytes 1048576
